TPU v7x, 32 devices: a whole 2x2x4 slice. The times are simulated.
32 devices in a mesh: sp: 8 (over z, x), tp: 4 (over y, core).
Axes of the slice: x: 2, y: 2, z: 4, core: 2. Of those that a mesh axis runs over, the one named last changes fastest.
Arguments:
- tokens: bfloat16 [4096, 2048], P(('sp', 'tp')), may hold values from -6 to 6
- input_gain: bfloat16 [2048], replicated, may hold values from 0.099609375 to 1.8984375
- weight_query: bfloat16 [2048, 1024], P(None, 'tp'), may hold values from -0.125 to 0.125
- weight_key: bfloat16 [2048, 1024], P(None, 'tp'), may hold values from -0.125 to 0.125
- weight_value: bfloat16 [2048, 2048], P(None, 'tp'), may hold values from -8 to 8
- weight_outgate: bfloat16 [2048, 2048], P(None, 'tp'), may hold values from -0.125 to 0.125
- weight_ingate: bfloat16 [2048, 8], replicated, may hold values from -0.125 to 0.125
- weight_forget: bfloat16 [2048, 8], replicated, may hold values from -0.125 to 0.125
- forget_shift: float32 [4096, 8], P('sp', 'tp'), may hold values from 0 to 20
- mem_gain: bfloat16 [2048], replicated, may hold values from 0.099609375 to 1.8984375
- query_down_weight: bfloat16 [2048, 768], P(None, 'tp'), may hold values from -0.125 to 0.125
- latent_down_weight: bfloat16 [2048, 512], P(None, 'tp'), may hold values from -0.125 to 0.125
- down_rotary: bfloat16 [2048, 64], replicated, may hold values from -0.125 to 0.125
- query_gain: float32 [768], replicated, may hold values from 0.15 to 12
- latent_gain: float32 [512], replicated, may hold values from 0.15 to 12
- query_up_weight: bfloat16 [768, 1536], P(None, 'tp'), may hold values from -0.4375 to 0.4375
- key_up_weight: bfloat16 [512, 1024], P(None, 'tp'), may hold values from -0.25 to 0.25
- value_up_weight: bfloat16 [512, 1024], P(None, 'tp'), may hold values from -0.25 to 0.25
- out_memory: bfloat16 [2048, 2048], P('tp'), may hold values from -0.5 to 0.5
- out_attend: bfloat16 [1024, 2048], P('tp'), may hold values from -0.75 to 0.75
Outputs:
- mixed: bfloat16 [4096, 2048], P(('sp', 'tp'))
All inputs are finite; a program needn't handle non-finite values.
Results may differ from a plain program's by a relative error of at most 0.04.
The roundings to bfloat16 on the way count: a program that leaves them out, or rounds other values in their place, can miss the bound.
Values may be sent and summed in bfloat16 or wider, within the bound.
A program may use at most 128 MiB of HBM per device.

v0:
```python
import math

import jax
import jax.numpy as jnp
from jax import lax
from jax.sharding import PartitionSpec as P

MEMORY_HEADS = 8
M_QK = 128
M_V = 256
PLAIN_CHANNELS = 128
ROTARY_CHANNELS = 64
VALUE_CHANNELS = 128
BLOCK = 64


SMALL_CONSTANT = 1e-06
SOFTCAP = 15.0
ROTARY_BASE = 10000.0
PRECISE = lax.Precision.HIGHEST
FAR_BELOW = -1e30


def carried_in(shard, axis, combine, identity):
    peers, index = (lax.axis_size(axis), lax.axis_index(axis))
    everything = jax.tree.map(lambda part: lax.all_gather(part, axis), shard)
    start = jax.tree.map(
        lambda part, zero: jnp.broadcast_to(jnp.asarray(zero, part.dtype), part.shape),
        shard,
        identity,
    )

    def step(k, before):
        reached = k < index
        new = combine(before, jax.tree.map(lambda part: part[k], everything))
        return jax.tree.map(lambda a, b: jnp.where(reached, a, b), new, before)

    return lax.fori_loop(0, peers, step, start)


def rms_scale(values, gain):
    widened = values.astype(jnp.float32)
    return (
        widened
        * lax.rsqrt(jnp.mean(widened * widened, axis=-1, keepdims=True) + SMALL_CONSTANT)
        * gain.astype(jnp.float32)
    )


def rotate(values, positions):
    halfway = values.shape[-1] // 2
    inverse = jnp.power(ROTARY_BASE, -jnp.arange(halfway, dtype=jnp.float32) / halfway)
    angles = positions.astype(jnp.float32)[:, None] * inverse
    cosine = jnp.cos(angles)
    sine_part = jnp.sin(angles)
    if values.ndim == 3:
        cosine = cosine[:, None, :]
        sine_part = sine_part[:, None, :]
    widened = values.astype(jnp.float32)
    first = widened[..., :halfway]
    second = widened[..., halfway:]
    turned = jnp.concatenate(
        [first * cosine - second * sine_part, second * cosine + first * sine_part], axis=-1
    )
    return turned.astype(jnp.bfloat16)


def update_state(carried, key_rows, value_rows, input_gate, cumulative):
    matrix, normal, stabilizer = carried
    last_total = cumulative[:, -1]
    weight_log = last_total[:, None] - cumulative + input_gate
    new_max = jnp.maximum(last_total + stabilizer, jnp.max(weight_log, axis=-1))
    weights = jnp.exp(weight_log - new_max[:, None])
    decay = jnp.exp(last_total + stabilizer - new_max)
    matrix = decay[:, None, None] * matrix + jnp.einsum(
        "hsv,hsd->hvd", weights[:, :, None] * value_rows, key_rows, precision=PRECISE
    )
    normal = decay[:, None] * normal + jnp.einsum(
        "hs,hsd->hd", weights, key_rows, precision=PRECISE
    )
    return (matrix, normal, new_max)


def block_step(carried, inputs):
    query_rows, key_rows, value_rows, input_gate, log_forget = inputs
    matrix, normal, stabilizer = carried
    cumulative = jnp.cumsum(log_forget, axis=-1)
    block_len = log_forget.shape[-1]
    causal = jnp.tril(jnp.ones((block_len, block_len), dtype=bool))
    pair_log = cumulative[:, :, None] - cumulative[:, None, :] + input_gate[:, None, :]
    pair_log = jnp.where(causal, pair_log, -jnp.inf)
    carried_log = cumulative + stabilizer[:, None]
    row_max = jnp.maximum(carried_log, jnp.max(pair_log, axis=-1))
    within = jnp.exp(pair_log - row_max[:, :, None])
    across = jnp.exp(carried_log - row_max)
    affinity = jnp.einsum("hjd,hsd->hjs", query_rows, key_rows, precision=PRECISE) * within
    numerator = jnp.einsum("hjs,hsv->hjv", affinity, value_rows, precision=PRECISE)
    numerator = numerator + across[:, :, None] * jnp.einsum(
        "hjd,hvd->hjv", query_rows, matrix, precision=PRECISE
    )
    denominator = jnp.sum(affinity, axis=-1) + across * jnp.einsum(
        "hjd,hd->hj", query_rows, normal, precision=PRECISE
    )
    output = numerator / jnp.maximum(jnp.abs(denominator), jnp.exp(-row_max))[:, :, None]
    return (update_state(carried, key_rows, value_rows, input_gate, cumulative), output)


def summary_step(carried, inputs):
    key_rows, value_rows, input_gate, log_forget = inputs
    return (
        update_state(carried, key_rows, value_rows, input_gate, jnp.cumsum(log_forget, axis=-1)),
        None,
    )


def merge_states(earlier, later):
    decayed = later[3] + earlier[2]
    joined = jnp.maximum(decayed, later[2])
    early_part = jnp.exp(decayed - joined)
    late_part = jnp.exp(later[2] - joined)
    return (
        early_part[:, None, None] * earlier[0] + late_part[:, None, None] * later[0],
        early_part[:, None] * earlier[1] + late_part[:, None] * later[1],
        joined,
        earlier[3] + later[3],
    )


def per_device(
    tokens,
    input_gain,
    weight_query,
    weight_key,
    weight_value,
    weight_outgate,
    weight_ingate,
    weight_forget,
    forget_shift,
    mem_gain,
    query_down_weight,
    latent_down_weight,
    down_rotary,
    query_gain,
    latent_gain,
    query_up_weight,
    key_up_weight,
    value_up_weight,
    out_memory,
    out_attend,
):
    normed = rms_scale(tokens, input_gain).astype(jnp.bfloat16)
    tp_index = lax.axis_index("tp")
    mem_heads = weight_query.shape[1] // M_QK
    att_heads = key_up_weight.shape[1] // PLAIN_CHANNELS
    ingate_cols = lax.dynamic_slice_in_dim(weight_ingate, tp_index * mem_heads, mem_heads, 1)
    forget_cols = lax.dynamic_slice_in_dim(weight_forget, tp_index * mem_heads, mem_heads, 1)
    weight_list = (
        weight_query,
        weight_key,
        weight_value,
        weight_outgate,
        query_down_weight,
        latent_down_weight,
        down_rotary,
        ingate_cols,
        forget_cols,
    )

    def project(portion):
        return jnp.concatenate(
            [
                jnp.dot(portion, weight, preferred_element_type=jnp.float32)
                for weight in weight_list
            ],
            axis=1,
        )

    projected = project(lax.all_gather(normed, "tp", axis=0, tiled=True))
    sections = []
    offset = 0
    for weight in weight_list:
        sections.append(projected[:, offset : offset + weight.shape[1]])
        offset = offset + weight.shape[1]
    stored = tuple((section.astype(jnp.bfloat16) for section in sections[:7]))
    mem_query, mem_key, mem_value, mem_outgate, query_latent, keyval_latent, key_raw = (
        lax.optimization_barrier(stored)
    )
    in_gate = SOFTCAP * jnp.tanh(sections[7] / SOFTCAP)
    log_forget = jax.nn.log_sigmoid(SOFTCAP * jnp.tanh((sections[8] + forget_shift) / SOFTCAP))
    length = projected.shape[0]
    positions = lax.axis_index("sp") * length + jnp.arange(length, dtype=jnp.int32)
    query_whole, latent_whole = (
        lax.all_gather(query_latent, "tp", axis=1, tiled=True),
        lax.all_gather(keyval_latent, "tp", axis=1, tiled=True),
    )
    normed_query = rms_scale(query_whole, query_gain).astype(jnp.bfloat16)
    normed_latent = rms_scale(latent_whole, latent_gain).astype(jnp.bfloat16)
    block_count = length // BLOCK

    def to_blocks(array, width):
        return (
            array.astype(jnp.float32)
            .reshape(block_count, BLOCK, mem_heads, width)
            .transpose(0, 2, 1, 3)
        )

    def gate_blocks(array):
        return array.reshape(block_count, BLOCK, mem_heads).transpose(0, 2, 1)

    query_blocks = to_blocks(mem_query, M_QK)
    key_blocks = to_blocks(mem_key, M_QK) * M_QK ** (-0.5)
    value_blocks = to_blocks(mem_value, M_V)
    ingate_blocks = gate_blocks(in_gate)
    forget_blocks = gate_blocks(log_forget)
    empty_state = (
        jnp.zeros((mem_heads, M_V, M_QK), jnp.float32),
        jnp.zeros((mem_heads, M_QK), jnp.float32),
        jnp.full((mem_heads,), FAR_BELOW, jnp.float32),
    )
    local_state, _ = lax.scan(
        summary_step, empty_state, (key_blocks, value_blocks, ingate_blocks, forget_blocks)
    )
    identity = empty_state + (jnp.zeros((mem_heads,), jnp.float32),)
    prefix = carried_in(
        (local_state[0], local_state[1], local_state[2], jnp.sum(log_forget, axis=0)),
        "sp",
        merge_states,
        identity,
    )
    start_max = jnp.maximum(prefix[3], prefix[2])
    rescale = jnp.exp(prefix[2] - start_max)
    initial = (prefix[0] * rescale[:, None, None], prefix[1] * rescale[:, None], start_max)
    _, cell = lax.scan(
        block_step, initial, (query_blocks, key_blocks, value_blocks, ingate_blocks, forget_blocks)
    )
    cell = cell.transpose(0, 2, 1, 3).reshape(length, mem_heads * M_V)
    cell_total = lax.psum(jnp.sum(cell * cell, axis=1), "tp")
    gain_part = lax.dynamic_slice_in_dim(mem_gain, tp_index * mem_heads * M_V, mem_heads * M_V, 0)
    gated = (
        cell
        * lax.rsqrt(cell_total / (MEMORY_HEADS * M_V) + SMALL_CONSTANT)[:, None]
        * gain_part.astype(jnp.float32)
    )
    gated = gated * jax.nn.sigmoid(mem_outgate.astype(jnp.float32))
    gated = gated.astype(jnp.bfloat16)
    query_all = jnp.dot(normed_query, query_up_weight, preferred_element_type=jnp.float32).astype(
        jnp.bfloat16
    )
    query_all = query_all.reshape(length, att_heads, PLAIN_CHANNELS + ROTARY_CHANNELS)
    query_nope = query_all[..., :PLAIN_CHANNELS]
    query_rot = rotate(query_all[..., PLAIN_CHANNELS:], positions)
    key_rot = rotate(key_raw, positions)
    factor = (PLAIN_CHANNELS + ROTARY_CHANNELS) ** (-0.5)

    def attend_block(carried, key_nope, key_rotary, value_rows, key_start):
        row_max, summed, accum = carried
        number = key_nope.shape[0]
        key_pos = key_start + jnp.arange(number, dtype=jnp.int32)
        scores = jnp.einsum(
            "qhd,khd->hqk",
            query_nope,
            key_nope.reshape(number, att_heads, PLAIN_CHANNELS),
            preferred_element_type=jnp.float32,
        )
        scores = (
            scores
            + jnp.einsum("qhd,kd->hqk", query_rot, key_rotary, preferred_element_type=jnp.float32)
        ) * factor
        allowed = key_pos[None, :] <= positions[:, None]
        scores = jnp.where(allowed[None], scores, -jnp.inf)
        new_max = jnp.maximum(row_max, jnp.max(scores, axis=-1))
        probs = jnp.exp(scores - new_max[:, :, None])
        shrink = jnp.exp(row_max - new_max)
        summed = summed * shrink + jnp.sum(probs, axis=-1)
        accum = accum * shrink[:, :, None] + jnp.einsum(
            "hqk,khd->hqd",
            probs.astype(jnp.bfloat16),
            value_rows.reshape(number, att_heads, VALUE_CHANNELS),
            preferred_element_type=jnp.float32,
        )
        return (new_max, summed, accum)

    initial_att = (
        jnp.full((att_heads, length), FAR_BELOW, jnp.float32),
        jnp.zeros((att_heads, length), jnp.float32),
        jnp.zeros((att_heads, length, VALUE_CHANNELS), jnp.float32),
    )
    carried = initial_att
    piece_rows = (
        lax.all_gather(normed_latent, "sp", axis=0, tiled=True),
        lax.all_gather(key_rot, "sp", axis=0, tiled=True),
    )
    number = piece_rows[0].shape[0]
    size = math.gcd(number, 1024)

    def one_block(state, block_number):
        begin = block_number * size
        sub_rows = tuple(
            (lax.dynamic_slice_in_dim(member, begin, size, 0) for member in piece_rows)
        )

        def compute(current):
            key_nope = jnp.dot(
                sub_rows[0], key_up_weight, preferred_element_type=jnp.float32
            ).astype(jnp.bfloat16)
            value_rows = jnp.dot(
                sub_rows[0], value_up_weight, preferred_element_type=jnp.float32
            ).astype(jnp.bfloat16)
            key_rotary = sub_rows[1]
            return attend_block(current, key_nope, key_rotary, value_rows, begin)

        return (
            lax.cond(begin <= positions[length - 1], compute, lambda current: current, state),
            None,
        )

    carried, _ = lax.scan(one_block, carried, jnp.arange(number // size, dtype=jnp.int32))
    attended = (carried[2] / carried[1][:, :, None]).astype(jnp.bfloat16)
    attended = attended.transpose(1, 0, 2).reshape(length, att_heads * VALUE_CHANNELS)
    return lax.psum_scatter(
        (
            jnp.dot(gated, out_memory, preferred_element_type=jnp.float32)
            + jnp.dot(attended, out_attend, preferred_element_type=jnp.float32)
        ).astype(jnp.bfloat16),
        "tp",
        scatter_dimension=0,
        tiled=True,
    )


def solution(mesh):
    placed = (
        P(("sp", "tp"), None),
        P(),
        P(None, "tp"),
        P(None, "tp"),
        P(None, "tp"),
        P(None, "tp"),
        P(),
        P(),
        P("sp", "tp"),
        P(),
        P(None, "tp"),
        P(None, "tp"),
        P(),
        P(),
        P(),
        P(None, "tp"),
        P(None, "tp"),
        P(None, "tp"),
        P("tp", None),
        P("tp", None),
    )
    return jax.shard_map(
        per_device, mesh=mesh, in_specs=placed, out_specs=P(("sp", "tp"), None), check_vma=False
    )
```

profile of v0, /device:TPU:26, one launch (start us, length us, event | category | flops | bytes accessed | tf_op | source)
XLA Modules:
  0.0 367.4 jit_solution(11637995545178317613)
XLA Ops:
  8.6 2.0 fusion.77
  10.8 23.6 %all-gather.9.cloned.1.call-done = bf16[512,2048]{1,0:T(8,128)(2,1)} async-done(((bf16[128,2048]{1,0:T(8,128)(2,1)}), bf16[512,2048]{1,0:T(8,128)(2,1)}) %all-gather.9.cloned.1.call-update) | async-done | bytes 2097168 | tf_op jit(solution)/shard_map/all_gather | solution.py:178
  34.3 4.5 %convolution_convert_fusion.2 = bf16[512,512]{1,0:T(8,128)(2,1)} fusion(bf16[512,2048]{1,0:T(8,128)(2,1)} %all-gather.9.cloned.1.call-done, bf16[2048,512]{1,0:T(8,128)(2,1)} %param.35), kind=kOutput, calls=%fused_computation.118 | convolution fusion | flops 1074003968 | bytes 4718592 | tf_op jit(solution)/shard_map/dot_general | solution.py:172
  38.8 2.0 convolution_convert_fusion.3
  47.5 2.0 reshape.315
  49.5 2.7 reshape.314
  52.2 2.5 copy.72
  56.3 2.2 fusion.70
  58.7 2.0 copy_bitcast_fusion.1
  60.7 20.5 %while.67 = (s32[]{:T(128)}, f32[2,256,128]{2,1,0:T(8,128)S(1)}, f32[2,128]{1,0:T(2,128)S(1)}, f32[2]{0:T(128)S(1)}, f32[8,2,64]{2,1,0:T(2,128)S(1)}, /*index=5*...) while((s32[]{:T(128)}, f32[2,256,128]{2,1,0:T(8,128)S(1)}, ...), condition=%wide.region_4.5_spmd.clone, body=%wide.region_1.0_spmd.clone.sunk | while | flops 50766984 | bytes 798945 | solution.py:220
  86.1 17.1 %all-reduce.2 = (f32[16]{0:T(128)S(1)}, f32[16]{0:T(128)S(1)}) all-reduce(f32[16]{0:T(128)S(1)} %negate_dynamic-update-slice_fusion, f32[16]{0:T(128)S(1)} %dynamic-update-slice.1), channel_id=2, replica_groups=mesh['sp'=8,'tp'=4] {'sp'}, use_global_device_ids=true, to_apply=%add | all-reduce | flops 32 | bytes 256
  103.9 8.0 %all_gather.47 = bf16[512,768]{0,1:T(8,128)(2,1)S(1)} all-gather(bf16[512,192]{0,1:T(8,128)(2,1)} %convolution_convert_fusion.7), channel_id=1, replica_groups=mesh['sp'=8,'tp'=4] {'tp'}, dimensions={1}, use_global_device_ids=true | all-gather | bytes 983040 | tf_op jit(solution)/shard_map/all_gather | solution.py:193
  112.1 1.7 convolution_convert_fusion.4
  114.8 18.7 %all-gather.4 = f32[8,2,128]{2,1,0:T(2,128)S(1)} all-gather(f32[1,2,128]{2,1,0:T(2,128)S(1)} %bitcast.240), channel_id=5, replica_groups=mesh['sp'=8,'tp'=4] {'sp'}, dimensions={0}, use_global_device_ids=true | all-gather | bytes 9216 | tf_op jit(solution)/shard_map/all_gather | solution.py:26
  135.5 7.3 %all_gather.45 = bf16[512,512]{1,0:T(8,128)(2,1)S(1)} all-gather(bf16[512,128]{1,0:T(8,128)(2,1)} %convolution_convert_fusion.8), channel_id=1, replica_groups=mesh['sp'=8,'tp'=4] {'tp'}, dimensions={1}, use_global_device_ids=true | all-gather | bytes 655360 | tf_op jit(solution)/shard_map/all_gather | solution.py:194
  143.0 33.4 %all_gather.48 = bf16[4096,64]{0,1:T(8,128)(2,1)} all-gather(bf16[512,64]{0,1:T(8,128)(2,1)S(1)} %pad_maximum_fusion.1), channel_id=1, replica_groups=mesh['sp'=8,'tp'=4] {'sp'}, dimensions={0}, use_global_device_ids=true | all-gather | bytes 589824 | tf_op jit(solution)/shard_map/all_gather | solution.py:291
  177.6 14.9 %while.68 = (s32[]{:T(128)}, f32[2,256,128]{2,1,0:T(8,128)S(1)}, f32[2,128]{1,0:T(2,128)S(1)}, f32[2]{0:T(128)S(1)}, f32[2]{0:T(128)S(1)}, /*index=5*/s32[]{:T(1...) while((s32[]{:T(128)}, f32[2,256,128]{2,1,0:T(8,128)S(1)}, ...), condition=%wide.region_7.8_spmd.clone, body=%wide.region_6.7_spmd.clone.sunk | while | flops 328984 | bytes 789781 | solution.py:38
  192.7 75.5 %while.65 = (s32[]{:T(128)}, f32[2,256,128]{2,1,0:T(8,128)S(1)}, f32[2,128]{1,0:T(2,128)S(1)}, f32[2]{0:T(128)S(1)}, f32[8,2,64,256]{3,2,1,0:T(8,128)}, /*index=...) while((s32[]{:T(128)}, f32[2,256,128]{2,1,0:T(8,128)S(1)}, ...), condition=%wide.region_13.14_spmd, body=%wide.region_8.13_spmd.sunk | while | flops 139163392 | bytes 1946349 | solution.py:233
  198.3 1.9 fusion.175
  207.7 1.9 fusion.175
  217.2 1.9 fusion.175
  226.6 1.9 fusion.175
  236.0 1.9 fusion.175
  245.4 1.9 fusion.175
  254.8 1.9 fusion.175
  264.3 1.9 fusion.175
  268.2 2.1 copy.53
  271.6 5.6 %psum.7 = f32[512]{0:T(512)S(1)} all-reduce(f32[512]{0:T(512)S(1)} %reduce_sum.71), channel_id=1, replica_groups=mesh['sp'=8,'tp'=4] {'tp'}, use_global_device_ids=true, to_apply=%region_15.16 | all-reduce | flops 512 | bytes 4096 | tf_op jit(solution)/shard_map/psum | solution.py:237
  277.9 46.2 %while.66 = (s32[]{:T(128)}, f32[2,512]{1,0:T(2,128)S(1)}, f32[2,512]{1,0:T(2,128)S(1)}, f32[2,512,128]{2,1,0:T(8,128)S(1)}, s32[4]{0:T(128)}, /*index=5*/s32[51...) while((s32[]{:T(128)}, f32[2,512]{1,0:T(2,128)S(1)}, ...), condition=%wide.region_23.24_spmd, body=%wide.region_18.23_spmd.sunk | while | flops 1217661952 | bytes 28387700 | solution.py:317
  280.8 8.5 %conditional.2 = ((f32[2,512]{1,0:T(2,128)S(1)}, f32[2,512]{1,0:T(2,128)S(1)}, f32[2,512,128]{2,1,0:T(8,128)S(1)})) conditional(s32[]{:T(128)} %convert_element_type.180, (f32[2,512]{1,0:T(2,128)S(1)}, f32[2,512]{1,0:T(2,128)S(1)}, f32[2,512,128]{2,1,0:T(8,128)S(1)}) %tuple.131, (s32[]{:T(128)}, s32[512]{0:T(512)S(1)}, ...), branch_computations={%region_19.19_spmd, %region_20.22_spmd} | conditional | flops 1217661952 | bytes 28387410 | solution.py:313
  280.9 1.7 convolution_convert_fusion.1
  283.7 2.1 fusion.100
  286.5 1.7 convolution_convert_fusion
  292.4 8.5 %conditional.2 = ((f32[2,512]{1,0:T(2,128)S(1)}, f32[2,512]{1,0:T(2,128)S(1)}, f32[2,512,128]{2,1,0:T(8,128)S(1)})) conditional(s32[]{:T(128)} %convert_element_type.180, (f32[2,512]{1,0:T(2,128)S(1)}, f32[2,512]{1,0:T(2,128)S(1)}, f32[2,512,128]{2,1,0:T(8,128)S(1)}) %tuple.131, (s32[]{:T(128)}, s32[512]{0:T(512)S(1)}, ...), branch_computations={%region_19.19_spmd, %region_20.22_spmd} | conditional | flops 1217661952 | bytes 28387410 | solution.py:313
  292.4 1.7 convolution_convert_fusion.1
  295.3 2.1 fusion.100
  298.0 1.7 convolution_convert_fusion
  303.9 8.6 %conditional.2 = ((f32[2,512]{1,0:T(2,128)S(1)}, f32[2,512]{1,0:T(2,128)S(1)}, f32[2,512,128]{2,1,0:T(8,128)S(1)})) conditional(s32[]{:T(128)} %convert_element_type.180, (f32[2,512]{1,0:T(2,128)S(1)}, f32[2,512]{1,0:T(2,128)S(1)}, f32[2,512,128]{2,1,0:T(8,128)S(1)}) %tuple.131, (s32[]{:T(128)}, s32[512]{0:T(512)S(1)}, ...), branch_computations={%region_19.19_spmd, %region_20.22_spmd} | conditional | flops 1217661952 | bytes 28387410 | solution.py:313
  303.9 1.7 convolution_convert_fusion.1
  306.8 2.1 fusion.100
  309.5 1.7 convolution_convert_fusion
  315.5 8.5 %conditional.2 = ((f32[2,512]{1,0:T(2,128)S(1)}, f32[2,512]{1,0:T(2,128)S(1)}, f32[2,512,128]{2,1,0:T(8,128)S(1)})) conditional(s32[]{:T(128)} %convert_element_type.180, (f32[2,512]{1,0:T(2,128)S(1)}, f32[2,512]{1,0:T(2,128)S(1)}, f32[2,512,128]{2,1,0:T(8,128)S(1)}) %tuple.131, (s32[]{:T(128)}, s32[512]{0:T(512)S(1)}, ...), branch_computations={%region_19.19_spmd, %region_20.22_spmd} | conditional | flops 1217661952 | bytes 28387410 | solution.py:313
  315.5 1.7 convolution_convert_fusion.1
  318.4 2.1 fusion.100
  321.1 1.7 convolution_convert_fusion
  324.3 2.1 fusion.104
  326.4 2.8 add_convert_fusion
  329.3 31.6 %reduce-scatter.2.cloned.1.call-done = bf16[128,2048]{1,0:T(8,128)(2,1)} async-done(((bf16[512,2048]{1,0:T(8,128)(2,1)}), bf16[128,2048]{1,0:T(8,128)(2,1)}) %reduce-scatter.2.cloned.1.call-update) | async-done | bytes 524304 | tf_op jit(solution)/shard_map/reduce_scatter | solution.py:320
  (391 shorter events, 136.5 us)
Async XLA Ops:
  6.5 319.9 %copy-start = (bf16[512,2048]{1,0:T(8,128)(2,1)S(1)}, bf16[512,2048]{1,0:T(8,128)(2,1)}, u32[]{:S(2)}) copy-start(bf16[512,2048]{1,0:T(8,128)(2,1)} %param.48) | copy-start | bytes 6291460
  6.5 27.8 %all-gather.9.cloned.1.call-start = ((), (), s32[]{:S(2)}) async-start(), calls=%async_computation.1 | async-start | bytes 2621440 | tf_op jit(solution)/shard_map/all_gather | solution.py:178
  10.7 166.9 %all-gather.13.cloned.1.call-start = ((), (), s32[]{:S(2)}) async-start(), calls=%async_computation.4 | async-start | bytes 2359296 | tf_op jit(solution)/shard_map/all_gather | solution.py:26
  34.3 4.5 %copy-start.1 = (bf16[512,2048]{1,0:T(8,128)(2,1)S(1)}, bf16[512,2048]{1,0:T(8,128)(2,1)}, u32[]{:S(2)}) copy-start(bf16[512,2048]{1,0:T(8,128)(2,1)} %all-gather.9.cloned.1.call-done) | copy-start | bytes 6291460
  34.3 4.5 %copy-start.18 = (bf16[2048,512]{1,0:T(8,128)(2,1)S(1)}, bf16[2048,512]{1,0:T(8,128)(2,1)}, u32[]{:S(2)}) copy-start(bf16[2048,512]{1,0:T(8,128)(2,1)} %param.34) | copy-start | bytes 6291460
  38.8 2.1 copy-start.19
  40.9 1.2 copy-start.20
  42.1 1.4 copy-start.21
  43.5 1.6 copy-start.8
  45.1 1.4 copy-start.10
  47.5 7.2 %copy-start.15 = (f32[512,2]{0,1:T(2,128)S(1)}, f32[512,2]{0,1:T(2,128)}, u32[]{:S(2)}) copy-start(f32[512,2]{0,1:T(2,128)} %param.38) | copy-start | bytes 12292
  52.2 2.5 copy-start.2
  60.7 21.4 %copy-start.23 = (u32[32]{0:T(128)S(1)}, u32[32]{0:T(128)}, u32[]{:S(2)}) copy-start(u32[32]{0:T(128)} %constant.164) | copy-start | bytes 388
  81.2 0.7 copy-start.3
  81.2 22.6 %copy-start.11 = (f32[8,2,64]{2,1,0:T(2,128)}, f32[8,2,64]{2,1,0:T(2,128)S(1)}, u32[]{:S(2)}) copy-start(f32[8,2,64]{2,1,0:T(2,128)S(1)} %get-tuple-element.1171) | copy-start | bytes 12292
  81.2 22.6 %copy-start.12 = (f32[8,2,64]{2,1,0:T(2,128)}, f32[8,2,64]{2,1,0:T(2,128)S(1)}, u32[]{:S(2)}) copy-start(f32[8,2,64]{2,1,0:T(2,128)S(1)} %get-tuple-element.1172) | copy-start | bytes 12292
  81.2 30.9 %copy-start.22 = (f32[768]{0:T(1024)S(1)}, f32[768]{0:T(1024)}, u32[]{:S(2)}) copy-start(f32[768]{0:T(1024)} %param.43) | copy-start | bytes 9220
  82.0 195.3 %all-gather.11.cloned.1.call-start = ((), (), s32[]{:S(2)}) async-start(), calls=%async_computation.2 | async-start | bytes 4718592 | tf_op jit(solution)/shard_map/all_gather | solution.py:290
  113.8 0.7 copy-start.9
  114.7 61.6 %copy-start.16 = (f32[512]{0:T(512)S(1)}, f32[512]{0:T(512)}, u32[]{:S(2)}) copy-start(f32[512]{0:T(512)} %param.44) | copy-start | bytes 6148
  135.4 42.2 %copy-start.13 = (f32[2]{0:T(128)S(1)}, f32[2]{0:T(128)}, u32[]{:S(2)}) copy-start(f32[2]{0:T(128)} %custom-call.5) | copy-start | bytes 28
  135.4 42.2 %copy-start.14 = (f32[2]{0:T(128)S(1)}, f32[2]{0:T(128)}, u32[]{:S(2)}) copy-start(f32[2]{0:T(128)} %custom-call.6) | copy-start | bytes 28
  177.4 183.5 %reduce-scatter.2.cloned.1.call-start = ((), (), s32[]{:S(2)}) async-start(), calls=%async_computation.3 | async-start | bytes 2621440 | tf_op jit(solution)/shard_map/reduce_scatter | solution.py:320
  268.2 3.2 copy-start.6
  270.3 7.5 %copy-start.4 = (bf16[512,256]{1,0:T(8,128)(2,1)S(1)}, bf16[512,256]{1,0:T(8,128)(2,1)}, u32[]{:S(2)}) copy-start(bf16[512,256]{1,0:T(8,128)(2,1)} %param.46) | copy-start | bytes 786436
  270.3 7.5 %copy-start.5 = (bf16[512,256]{1,0:T(8,128)(2,1)S(1)}, bf16[512,256]{1,0:T(8,128)(2,1)}, u32[]{:S(2)}) copy-start(bf16[512,256]{1,0:T(8,128)(2,1)} %param.47) | copy-start | bytes 786436
  324.3 2.1 copy-start.7
  324.3 2.1 copy-start.17
  324.3 2.1 copy-start.24
Sparse Core Ops, SparseCore 0:
  10.8 23.5 all-gather.8
  82.1 46.8 all-gather.12
  177.5 70.6 all-gather.10
  329.4 31.4 reduce-scatter.1
where the time goes:
time: 373 us; the launch traced here: 367 us
  matrix products  123 us (33%)
  blocking collectives  90 us (24%)
  waiting for transfers between devices  55.3 us (15%)
  other arithmetic  45.9 us (12%)
  local copies, waits for them, and re-layouts  32.9 us (9%)
  between operations  14.3 us (4%)
  loops' own time  5.56 us (1%)
    all_gather x1, blocking collectives, per_device(): lax.all_gather(key_rot, 'sp', axis=0, tiled=True)  33.4 us
    reduce_scatter x1, waiting for transfers between devices, per_device(): lax.psum_scatter((jnp.dot(gated, out_memory, preferred_element_type=jnp.f...  31.6 us
    dot_general x16, matrix products, update_state(): jnp.einsum('hsv,hsd->hvd', weights[:, :, None] * value_rows, key_rows, pr...  25.6 us
    all_gather x1, waiting for transfers between devices, per_device(): projected = project(lax.all_gather(normed, 'tp', axis=0, tiled=True))  23.6 us
    all_gather x1, blocking collectives, carried_in(): everything = jax.tree.map(lambda part: lax.all_gather(part, axis), shard)  18.7 us
    unnamed x1, blocking collectives  17.1 us
    dot_general x9, matrix products, project(): jnp.dot(portion, weight, preferred_element_type=jnp.float32)  16.1 us
    dot_general x8, matrix products, block_step(): jnp.einsum('hjs,hsv->hjv', affinity, value_rows, precision=PRECISE)  15.1 us
  transfers between devices with their start and end apart: 4, of which 2 were waited for; matrix products, arithmetic and copies ran while one was open for 28% of the time, Pallas kernels for 0%

commit v1 on v0

v1 whole, which is shorter than its diff:
```python
import functools
import math

import jax
import jax.numpy as jnp
from jax import lax
from jax.experimental import pallas as pl
from jax.experimental.pallas import tpu as pltpu
from jax.sharding import PartitionSpec as P

MEMORY_HEADS = 8
M_QK = 128
M_V = 256
PLAIN_CHANNELS = 128
ROTARY_CHANNELS = 64
VALUE_CHANNELS = 128
HEAD_WIDTH = PLAIN_CHANNELS + ROTARY_CHANNELS
SMALL_CONSTANT = 1e-06
SOFTCAP = 15.0
ROTARY_BASE = 10000.0
FAR_BELOW = -1e30
EXTRA_ROWS = 16
F32 = jnp.float32
BF16 = jnp.bfloat16
VMEM_LIMIT = 56 * 1024 * 1024
NT = (((1,), (1,)), ((), ()))
TN = (((0,), (0,)), ((), ()))


def dot(a, b):
    return jnp.dot(a, b, preferred_element_type=F32)


def rms_scale(values, gain):
    widened = values.astype(F32)
    return (
        widened
        * lax.rsqrt(jnp.mean(widened * widened, axis=-1, keepdims=True) + SMALL_CONSTANT)
        * gain.astype(F32)
    )


def split3(value):
    high = value.astype(BF16)
    rest = value - high.astype(F32)
    middle = rest.astype(BF16)
    low = (rest - middle.astype(F32)).astype(BF16)
    return high, middle, low


def local_memory(heads, query_ref, key_ref, value_ref, small_ref, shift_ref,
                 num_ref, stats_ref, state_ref, extra_ref):
    length = query_ref.shape[0]
    scale = M_QK ** -0.5
    gate = small_ref[:, ROTARY_CHANNELS:ROTARY_CHANNELS + heads]
    forget = small_ref[:, ROTARY_CHANNELS + heads:ROTARY_CHANNELS + 2 * heads] + shift_ref[...]
    gate = SOFTCAP * jnp.tanh(gate / SOFTCAP)
    capped = SOFTCAP * jnp.tanh(forget / SOFTCAP)
    log_forget = jnp.minimum(capped, 0.0) - jnp.log1p(jnp.exp(-jnp.abs(capped)))
    row = lax.broadcasted_iota(jnp.int32, (length, length), 0)
    col = lax.broadcasted_iota(jnp.int32, (length, length), 1)
    causal = col <= row
    cumulative = jnp.dot(
        causal.astype(F32), log_forget, preferred_element_type=F32,
        precision=lax.Precision.HIGHEST,
    )
    offset = gate - cumulative
    lanes = jnp.concatenate(
        [offset, jnp.zeros((length, 128 - heads), F32)], axis=1
    )
    offset_rows = lanes.T
    stats = []
    extras = []
    for h in range(heads):
        q = query_ref[:, h * M_QK:(h + 1) * M_QK]
        k = key_ref[:, h * M_QK:(h + 1) * M_QK]
        v = value_ref[:, h * M_V:(h + 1) * M_V]
        b = cumulative[:, h:h + 1]
        w = offset_rows[h:h + 1, :]
        masked = jnp.where(causal, w, -jnp.inf)
        top = jnp.max(masked, axis=1, keepdims=True)
        weight = jnp.exp(masked - top)
        affinity = lax.dot_general(q, k, NT, preferred_element_type=F32) * (weight * scale)
        num_ref[:, h * M_V:(h + 1) * M_V] = dot(affinity.astype(BF16), v)
        stats += [b, b + top, jnp.sum(affinity, axis=1, keepdims=True)]
        last = b[length - 1:length, :]
        best = top[length - 1:length, :]
        decay = jnp.exp(offset[:, h:h + 1] - best) * scale
        state_ref[h * M_V:(h + 1) * M_V, :] = lax.dot_general(
            (decay * v.astype(F32)).astype(BF16), k, TN, preferred_element_type=F32
        ).astype(BF16)
        normal = jnp.sum(decay * k.astype(F32), axis=0, keepdims=True)
        parts = split3(normal) + split3(jnp.broadcast_to(last + best, (1, 128))) + split3(
            jnp.broadcast_to(last, (1, 128))
        )
        extras += [part.astype(F32) for part in parts]
    stats_ref[...] = jnp.concatenate(
        stats + [jnp.zeros((length, 128 - 3 * heads), F32)], axis=1
    )
    count = len(extras)
    rows = extra_ref.shape[0]
    extra_ref[...] = jnp.concatenate(
        extras + [jnp.zeros((rows - count, 128), F32)], axis=0
    ).astype(BF16)


def rotated(values, cosine, sine):
    half = values.shape[-1] // 2
    widened = values.astype(F32)
    first = widened[:, :half]
    second = widened[:, half:]
    return jnp.concatenate(
        [first * cosine - second * sine, second * cosine + first * sine], axis=1
    ).astype(BF16)


def prepare(heads, latents_ref, small_ref, cos_ref, sin_ref, qgain_ref, lgain_ref,
            qup_ref, kup_ref, vup_ref, state_ref, extra_ref, query_ref, pack_ref):
    shares, length, _ = latents_ref.shape
    lat_part = lgain_ref.shape[1]
    q_part = qgain_ref.shape[1]
    lat_sum = 0.0
    q_sum = 0.0
    for t in range(shares):
        a = latents_ref[t, :, :lat_part].astype(F32)
        b = latents_ref[t, :, lat_part:].astype(F32)
        lat_sum = lat_sum + jnp.sum(a * a, axis=1, keepdims=True)
        q_sum = q_sum + jnp.sum(b * b, axis=1, keepdims=True)
    lat_rs = lax.rsqrt(lat_sum / (shares * lat_part) + SMALL_CONSTANT)
    q_rs = lax.rsqrt(q_sum / (shares * q_part) + SMALL_CONSTANT)
    query = 0.0
    keys = 0.0
    values = 0.0
    for t in range(shares):
        a = latents_ref[t, :, :lat_part].astype(F32)
        b = latents_ref[t, :, lat_part:].astype(F32)
        a = (a * lat_rs * lgain_ref[t:t + 1, :]).astype(BF16)
        b = (b * q_rs * qgain_ref[t:t + 1, :]).astype(BF16)
        query = query + dot(b, qup_ref[t * q_part:(t + 1) * q_part, :])
        keys = keys + dot(a, kup_ref[t * lat_part:(t + 1) * lat_part, :])
        values = values + dot(a, vup_ref[t * lat_part:(t + 1) * lat_part, :])
    query = query.astype(BF16)
    cosine = cos_ref[...]
    sine = sin_ref[...]
    for h in range(heads):
        base = h * HEAD_WIDTH
        query_ref[h, :, :PLAIN_CHANNELS] = query[:, base:base + PLAIN_CHANNELS]
        query_ref[h, :, PLAIN_CHANNELS:] = rotated(
            query[:, base + PLAIN_CHANNELS:base + HEAD_WIDTH], cosine, sine
        )
    width_k = keys.shape[1]
    width_v = values.shape[1]
    pack_ref[:length, :width_k] = keys.astype(BF16)
    pack_ref[:length, width_k:width_k + width_v] = values.astype(BF16)
    base = width_k + width_v
    filled = state_ref.shape[0]
    pack_ref[:filled, base:base + 128] = state_ref[...]
    if filled < length:
        pack_ref[filled:length, base:base + 128] = jnp.zeros((length - filled, 128), BF16)
    pack_ref[:length, base + 128:] = rotated(
        small_ref[:, :ROTARY_CHANNELS].astype(BF16), cosine, sine
    )
    rows = extra_ref.shape[0]
    pack_ref[length:, :] = jnp.zeros((rows, pack_ref.shape[1]), BF16)
    pack_ref[length:, :128] = extra_ref[...]


def mixers(mem_heads, att_heads, where_ref, pack_ref, query_ref, memq_ref, num_ref, stats_ref,
           cell_ref, square_ref, attended_ref,
           top_ref, sum_ref, acc_ref, matrix_ref, normal_ref, stab_ref):
    step = pl.program_id(0)
    mine = where_ref[0]
    length = query_ref.shape[1]
    factor = HEAD_WIDTH ** -0.5
    width_k = att_heads * PLAIN_CHANNELS
    width_v = att_heads * VALUE_CHANNELS
    base = width_k + width_v

    @pl.when(step == 0)
    def _():
        top_ref[...] = jnp.full(top_ref.shape, FAR_BELOW, F32)
        sum_ref[...] = jnp.zeros(sum_ref.shape, F32)
        acc_ref[...] = jnp.zeros(acc_ref.shape, F32)
        matrix_ref[...] = jnp.zeros(matrix_ref.shape, F32)
        normal_ref[...] = jnp.zeros(normal_ref.shape, F32)
        stab_ref[...] = jnp.zeros(stab_ref.shape, F32)

    def attend(masked):
        rotary = pack_ref[0, :length, base + 128:]
        for h in range(att_heads):
            key = jnp.concatenate(
                [pack_ref[0, :length, h * PLAIN_CHANNELS:(h + 1) * PLAIN_CHANNELS], rotary], axis=1
            )
            scores = lax.dot_general(query_ref[h], key, NT, preferred_element_type=F32)
            if masked:
                row = lax.broadcasted_iota(jnp.int32, scores.shape, 0)
                col = lax.broadcasted_iota(jnp.int32, scores.shape, 1)
                scores = jnp.where(col <= row, scores, FAR_BELOW)
            old = top_ref[h, :, :1]
            new = jnp.maximum(old, jnp.max(scores, axis=1, keepdims=True))
            probs = jnp.exp((scores - new) * factor)
            shrink = jnp.exp((old - new) * factor)
            sum_ref[h] = sum_ref[h] * shrink + jnp.sum(probs, axis=1, keepdims=True)
            value = pack_ref[0, :length, width_k + h * VALUE_CHANNELS:width_k + (h + 1) * VALUE_CHANNELS]
            acc_ref[h] = acc_ref[h] * shrink + dot(probs.astype(BF16), value)
            top_ref[h] = jnp.broadcast_to(new, top_ref.shape[1:])

    @pl.when(step < mine)
    def _():
        attend(False)
        extra = pack_ref[0, length:, :128].astype(F32)
        state = pack_ref[0, :length, base:base + 128].astype(F32)
        pieces = [extra[9 * h + 3 * g:9 * h + 3 * g + 1] + extra[9 * h + 3 * g + 1:9 * h + 3 * g + 2]
                  + extra[9 * h + 3 * g + 2:9 * h + 3 * g + 3]
                  for h in range(mem_heads) for g in range(3)]
        for h in range(mem_heads):
            normal, best, last = pieces[3 * h:3 * h + 3]
            decayed = stab_ref[h:h + 1, :] + last
            new = jnp.maximum(decayed, best)
            early = jnp.exp(decayed - new)
            late = jnp.exp(best - new)
            rows = slice(h * M_V, (h + 1) * M_V)
            matrix_ref[rows, :] = matrix_ref[rows, :] * early + late * state[rows, :]
            normal_ref[h:h + 1, :] = normal_ref[h:h + 1, :] * early + late * normal
            stab_ref[h:h + 1, :] = new

    @pl.when(step == mine)
    def _():
        attend(True)
        for h in range(att_heads):
            attended_ref[:, h * VALUE_CHANNELS:(h + 1) * VALUE_CHANNELS] = (
                acc_ref[h] / sum_ref[h]
            ).astype(BF16)
        squares = 0.0
        for h in range(mem_heads):
            b = stats_ref[:, 3 * h:3 * h + 1]
            local = stats_ref[:, 3 * h + 1:3 * h + 2]
            local_den = stats_ref[:, 3 * h + 2:3 * h + 3]
            q = memq_ref[:, h * M_QK:(h + 1) * M_QK]
            carried = b + stab_ref[h:h + 1, :1]
            row_max = jnp.maximum(carried, local)
            across = jnp.exp(carried - row_max)
            within = jnp.exp(local - row_max)
            inter = lax.dot_general(
                q, matrix_ref[h * M_V:(h + 1) * M_V, :].astype(BF16), NT,
                preferred_element_type=F32,
            )
            dots = jnp.sum(q.astype(F32) * normal_ref[h:h + 1, :], axis=1, keepdims=True)
            den = within * local_den + across * dots
            den = jnp.maximum(jnp.abs(den), jnp.exp(-row_max))
            cell = (within * num_ref[:, h * M_V:(h + 1) * M_V] + across * inter) / den
            cell_ref[:, h * M_V:(h + 1) * M_V] = cell
            squares = squares + jnp.sum(cell * cell, axis=1, keepdims=True)
        square_ref[...] = squares


def params(**more):
    return pltpu.CompilerParams(vmem_limit_bytes=VMEM_LIMIT, **more)


def per_device(
    tokens, input_gain, weight_query, weight_key, weight_value, weight_outgate, weight_ingate,
    weight_forget, forget_shift, mem_gain, query_down_weight, latent_down_weight, down_rotary,
    query_gain, latent_gain, query_up_weight, key_up_weight, value_up_weight, out_memory,
    out_attend,
):
    tp_index = lax.axis_index("tp")
    tp = lax.axis_size("tp")
    sp = lax.axis_size("sp")
    mem_heads = weight_query.shape[1] // M_QK
    att_heads = key_up_weight.shape[1] // PLAIN_CHANNELS
    length = tokens.shape[0] * tp
    model = tokens.shape[1]
    ingate_cols = lax.dynamic_slice_in_dim(weight_ingate, tp_index * mem_heads, mem_heads, 1)
    forget_cols = lax.dynamic_slice_in_dim(weight_forget, tp_index * mem_heads, mem_heads, 1)
    small_weight = jnp.concatenate(
        [down_rotary, ingate_cols, forget_cols,
         jnp.zeros((model, 128 - ROTARY_CHANNELS - 2 * mem_heads), BF16)], axis=1
    )
    latent_weight = jnp.concatenate([latent_down_weight, query_down_weight], axis=1)
    positions = lax.axis_index("sp") * length + jnp.arange(length, dtype=jnp.int32)
    half = ROTARY_CHANNELS // 2
    inverse = jnp.power(ROTARY_BASE, -jnp.arange(half, dtype=F32) / half)
    angles = positions.astype(F32)[:, None] * inverse
    cosine = jnp.cos(angles)
    sine = jnp.sin(angles)

    normed = rms_scale(tokens, input_gain).astype(BF16)
    rows = lax.all_gather(normed, "tp", axis=0, tiled=True)
    latents = dot(rows, latent_weight).astype(BF16)
    latents_all = lax.all_gather(latents, "tp", axis=0)
    small = dot(rows, small_weight)
    mem_query = dot(rows, weight_query).astype(BF16)
    mem_key = dot(rows, weight_key).astype(BF16)
    mem_value = dot(rows, weight_value).astype(BF16)
    mem_outgate = dot(rows, weight_outgate).astype(BF16)

    extra_rows = -(-9 * mem_heads // 32) * 32
    num, stats, state, extra = pl.pallas_call(
        functools.partial(local_memory, mem_heads),
        out_shape=(
            jax.ShapeDtypeStruct((length, mem_heads * M_V), F32),
            jax.ShapeDtypeStruct((length, 128), F32),
            jax.ShapeDtypeStruct((mem_heads * M_V, 128), BF16),
            jax.ShapeDtypeStruct((extra_rows, 128), BF16),
        ),
        compiler_params=params(),
        name="local_memory",
    )(mem_query, mem_key, mem_value, small, forget_shift)

    width = att_heads * (PLAIN_CHANNELS + VALUE_CHANNELS) + 128 + ROTARY_CHANNELS
    query, pack = pl.pallas_call(
        functools.partial(prepare, att_heads),
        out_shape=(
            jax.ShapeDtypeStruct((att_heads, length, HEAD_WIDTH), BF16),
            jax.ShapeDtypeStruct((length + extra_rows, width), BF16),
        ),
        compiler_params=params(),
        name="prepare",
    )(
        latents_all, small, cosine, sine, query_gain.reshape(tp, -1), latent_gain.reshape(tp, -1),
        query_up_weight, key_up_weight, value_up_weight, state, extra,
    )
    packs = lax.all_gather(pack, "sp", axis=0)

    full = lambda shape: pl.BlockSpec(shape, lambda i, w: (0,) * len(shape))
    cell, squares, attended = pl.pallas_call(
        functools.partial(mixers, mem_heads, att_heads),
        grid_spec=pltpu.PrefetchScalarGridSpec(
            num_scalar_prefetch=1,
            grid=(sp,),
            in_specs=[
                pl.BlockSpec((1, length + extra_rows, width),
                             lambda i, w: (jnp.minimum(i, w[0]), 0, 0)),
                full(query.shape), full(mem_query.shape), full(num.shape), full(stats.shape),
            ],
            out_specs=[full((length, mem_heads * M_V)), full((length, 1)),
                       full((length, att_heads * VALUE_CHANNELS))],
            scratch_shapes=[
                pltpu.VMEM((att_heads, length, 128), F32),
                pltpu.VMEM((att_heads, length, 128), F32),
                pltpu.VMEM((att_heads, length, VALUE_CHANNELS), F32),
                pltpu.VMEM((mem_heads * M_V, 128), F32),
                pltpu.VMEM((8, 128), F32),
                pltpu.VMEM((8, 128), F32),
            ],
        ),
        out_shape=(
            jax.ShapeDtypeStruct((length, mem_heads * M_V), F32),
            jax.ShapeDtypeStruct((length, 1), F32),
            jax.ShapeDtypeStruct((length, att_heads * VALUE_CHANNELS), BF16),
        ),
        compiler_params=params(dimension_semantics=("arbitrary",)),
        name="mixers",
    )(lax.axis_index("sp").astype(jnp.int32).reshape(1), packs, query, mem_query, num, stats)

    total = lax.psum(squares, "tp")
    gain_part = lax.dynamic_slice_in_dim(mem_gain, tp_index * mem_heads * M_V, mem_heads * M_V, 0)
    gated = (
        cell * lax.rsqrt(total / (tp * mem_heads * M_V) + SMALL_CONSTANT) * gain_part.astype(F32)
        * jax.nn.sigmoid(mem_outgate.astype(F32))
    ).astype(BF16)
    partial = (dot(gated, out_memory) + dot(attended, out_attend)).astype(BF16)
    return lax.psum_scatter(partial, "tp", scatter_dimension=0, tiled=True)


def solution(mesh):
    placed = (
        P(("sp", "tp"), None), P(), P(None, "tp"), P(None, "tp"), P(None, "tp"), P(None, "tp"),
        P(), P(), P("sp", "tp"), P(), P(None, "tp"), P(None, "tp"), P(), P(), P(),
        P(None, "tp"), P(None, "tp"), P(None, "tp"), P("tp", None), P("tp", None),
    )
    return jax.shard_map(
        per_device, mesh=mesh, in_specs=placed, out_specs=P(("sp", "tp"), None), check_vma=False
    )
```

time: 373 us -> 256 us (0.69)
  matrix products: 123 us -> 22.7 us
  waiting for transfers between devices: 55.3 us -> 154 us
  blocking collectives: 90 us -> 15.1 us
  other arithmetic: 45.9 us -> 6.85 us
  Pallas kernels: 0 us -> 35.5 us
  local copies, waits for them, and re-layouts: 32.9 us -> 5.68 us
  loops' own time: 5.56 us -> 0 us
    dot_general x96 -> x7, matrix products: 123 us -> 22.7 us  [dot(): return jnp.dot(a, b, preferred_element_type=F32)]
    all_gather x3, waiting for transfers between devices: 23.6 us -> 123 us  [the longest x1 99.8 us: per_device(): packs = lax.all_gather(pack, 'sp', axis=0)]
    all_gather x4 -> x0, blocking collectives: 67.3 us -> none  [the longest x1 33.4 us: per_device(): lax.all_gather(key_rot, 'sp', axis=0, tiled=True)]
    pallas_call x0 -> x3, Pallas kernels: none -> 35.5 us  [the longest x1 24.6 us: per_device(): pl.pallas_call(functools.partial(mixers, mem_heads, att_heads), grid_spec...]
    unnamed x1 -> x0, blocking collectives: 17.1 us -> none
    select_n x24 -> x0, other arithmetic: 14.7 us -> none  [step(): return jax.tree.map(lambda a, b: jnp.where(reached, a, b), new, before)]
    transpose x6 -> x0, local copies, waits for them, and re-layouts: 11.3 us -> none  [the longest x4 9.16 us: to_blocks(): return array.astype(jnp.float32).reshape(block_count, BLOCK, mem_heads, w...]
    psum x1, blocking collectives: 5.63 us -> 15.1 us  [per_device(): total = lax.psum(squares, 'tp')]
  transfers between devices with their start and end apart: 4 -> 4, of which waited for: 2 -> 4; matrix products, arithmetic and copies ran while one was open for 28% -> 5% of each run, Pallas kernels for 0% -> 2%
where the time goes in v1:
time: 256 us; the launch traced here: 254 us
  waiting for transfers between devices  154 us (60%)
  Pallas kernels  35.5 us (14%)
  matrix products  22.7 us (9%)
  blocking collectives  15.1 us (6%)
  between operations  13.2 us (5%)
  other arithmetic  6.85 us (3%)
  local copies, waits for them, and re-layouts  5.68 us (2%)
    all_gather x1, waiting for transfers between devices, per_device(): packs = lax.all_gather(pack, 'sp', axis=0)  99.8 us
    reduce_scatter x1, waiting for transfers between devices, per_device(): return lax.psum_scatter(partial, 'tp', scatter_dimension=0, tiled=True)  31.6 us
    pallas_call x1, Pallas kernels, per_device(): pl.pallas_call(functools.partial(mixers, mem_heads, att_heads), grid_spec...  24.6 us
    dot_general x7, matrix products, dot(): return jnp.dot(a, b, preferred_element_type=F32)  22.7 us
    all_gather x1, waiting for transfers between devices, per_device(): rows = lax.all_gather(normed, 'tp', axis=0, tiled=True)  21.8 us
    psum x1, blocking collectives, per_device(): total = lax.psum(squares, 'tp')  15.1 us
    pallas_call x1, Pallas kernels, per_device(): pl.pallas_call(functools.partial(local_memory, mem_heads), out_shape=(jax...  5.91 us
  transfers between devices with their start and end apart: 4, of which 4 were waited for; matrix products, arithmetic and copies ran while one was open for 5% of the time, Pallas kernels for 2%

profile of v1, /device:TPU:26, one launch (start us, length us, event | category | flops | bytes accessed | tf_op | source)
XLA Modules:
  0.0 253.9 jit_solution(3542728798048232236)
XLA Ops:
  6.5 0.0 copy-start
  6.5 0.0 copy-start.3
  6.5 0.0 copy-start.2
  6.5 0.0 all-gather.6.cloned.1.call-start
  6.6 0.8 convert_element_type.44
  7.4 1.2 fusion.14
  8.7 2.0 fusion.16
  10.7 0.0 all-gather.6.cloned.1.call-update
  10.7 0.0 all-gather.8.cloned.1.call-start
  10.8 0.0 copy-done.3
  10.8 0.8 copy.30.shift_ref
  11.6 0.0 copy-done.2
  11.6 0.2 copy.27
  11.9 0.0 copy-done.4
  11.9 0.7 reshape.31.qgain_ref
  12.5 0.1 pad.3.clone
  12.6 21.8 %all-gather.6.cloned.1.call-done = bf16[512,2048]{1,0:T(8,128)(2,1)} async-done(((bf16[128,2048]{1,0:T(8,128)(2,1)}), bf16[512,2048]{1,0:T(8,128)(2,1)}) %all-gather.6.cloned.1.call-update) | async-done | bytes 2097168 | tf_op jit(solution)/shard_map/all_gather | solution.py:289
  34.4 3.4 %fusion.11 = bf16[512,320]{0,1:T(8,128)(2,1)} fusion(bf16[512,2048]{1,0:T(8,128)(2,1)} %all-gather.6.cloned.1.call-done, bf16[2048,192]{0,1:T(8,128)(2,1)} %param.30, bf16[2048,128]{0,1:T(8,128)(2,1)S(1)} %copy.27), kind=kOutput, calls=%fused_computation.16 | convolution fusion | flops 673873920 | bytes 3735552 | tf_op jit(solution)/shard_map/dot_general | solution.py:31
  37.7 0.0 all-gather.8.cloned.1.call-update
  37.8 0.0 all-gather.10.cloned.1.call-start
  37.9 0.8 constant_dynamic-slice_fusion
  38.7 1.8 multiply_sine_fusion
  40.5 0.0 copy-done.9
  40.5 3.3 %fusion.17.small_ref = f32[512,128]{1,0:T(8,128)} fusion(bf16[512,2048]{1,0:T(8,128)(2,1)} %all-gather.6.cloned.1.call-done, bf16[2048,2]{0,1:T(2,128)(2,1)S(1)} %get-tuple-element.25, bf16[2048,2]{0,1:T(2,128)(2,1)S(1)} %get-tuple-element.26, bf16[2048,64]{0,1:T(8,128)(2,1)S(1)} %copy-done.9, bf16[128]{0:T(256)(128)(2,1)S(1)} %pad.3.clone), kind=kOutput, calls=%fused_computation.22 | convolution fusion | flops 270532608 | bytes 2638080 | tf_op jit(solution)/shard_map/dot_general | solution.py:31
  43.7 0.0 copy-done.6
  43.7 0.0 copy-done.7
  43.8 1.4 convolution_convert_fusion.3.query_ref.memq_ref
  45.2 0.0 copy-done.8
  45.2 1.4 convolution_convert_fusion.2.key_ref
  46.6 0.5 copy-done.5
  47.1 2.0 convolution_convert_fusion.1.value_ref
  49.1 5.9 %local_memory.1 = (f32[512,512]{1,0:T(8,128)}, f32[512,128]{1,0:T(8,128)}, bf16[512,128]{1,0:T(8,128)(2,1)}, bf16[32,128]{1,0:T(8,128)(2,1)}) custom-call(bf16[512,256]{1,0:T(8,128)(2,1)} %convolution_convert_fusion.3.query_ref.memq_ref, bf16[512,256]{1,0:T(8,128)(2,1)} %convolution_convert_fusion.2.key_ref, ...), custom_call_target="tpu_custom_call" | custom-call | tf_op jit(solution)/shard_map/local_memory/pallas_call | solution.py:299
  55.0 1.1 all-gather.8.cloned.1.call-done
  56.1 2.6 %copy.28 = bf16[2048,320]{1,0:T(8,128)(2,1)} copy(bf16[2048,320]{0,1:T(8,128)(2,1)} %all-gather.8.cloned.1.call-done) | data formatting | bytes 2621440 | tf_op jit(solution)/shard_map/all_gather | solution.py:291
  58.7 5.0 %prepare.1 = (bf16[2,512,192]{2,1,0:T(8,128)(2,1)}, bf16[544,704]{1,0:T(8,128)(2,1)}) custom-call(bf16[4,512,320]{2,1,0:T(8,128)(2,1)} %bitcast.18, f32[512,128]{1,0:T(8,128)} %fusion.17.small_ref, f32[512,32]{1,0:T(8,128)} %get-tuple-element.24.cos_ref, f32[512,32]{1,0:T(8,128)} %get-tuple-element.23.sin_ref, f32[4,192]{1,0:T(4,128)} %reshape.31.qgain_ref, ...), custom_call_target="tpu_custom_call" | custom-call | tf_op jit(solution)/shard_map/prepare/pallas_call | solution.py:312
  63.7 0.0 all-gather.10.cloned.1.call-update
  63.7 0.2 reduce-scatter.2.cloned.1.call-start
  63.9 0.8 dynamic-slice_convert_fusion
  64.7 99.8 %all-gather.10.cloned.1.call-done = bf16[4352,704]{1,0:T(8,128)(2,1)} async-done(((bf16[544,704]{1,0:T(8,128)(2,1)}), bf16[4352,704]{1,0:T(8,128)(2,1)}) %all-gather.10.cloned.1.call-update) | async-done | bytes 6127632 | tf_op jit(solution)/shard_map/all_gather | solution.py:324
  164.5 24.6 %mixers.1 = (f32[512,512]{1,0:T(8,128)}, f32[512,1]{1,0:T(8,128)}, bf16[512,256]{1,0:T(8,128)(2,1)}) custom-call(s32[1]{0:T(128)} %bitcast.where_ref, bf16[8,544,704]{2,1,0:T(8,128)(2,1)} %bitcast.17, bf16[2,512,192]{2,1,0:T(8,128)(2,1)} %get-tuple-element.17.query_ref, bf16[512,256]{1,0:T(8,128)(2,1)} %convolution_convert_fusion.3.query_ref.memq_ref, ...), custom_call_target="tpu_custom_call" | custom-call | tf_op jit(solution)/shard_map/mixers/pallas_call | solution.py:327
  189.1 15.1 %psum.7 = f32[512,1]{1,0:T(8,128)S(1)} all-reduce(f32[512,1]{1,0:T(8,128)} %get-tuple-element.21), channel_id=1, replica_groups=mesh['sp'=8,'tp'=4] {'tp'}, use_global_device_ids=true, to_apply=%region_1.0 | all-reduce | flops 512 | bytes 4096 | tf_op jit(solution)/shard_map/psum | solution.py:357
  204.3 0.2 rsqrt_reduce_fusion
  204.4 0.0 copy-done.1
  204.4 3.6 %fusion.31 = f32[512,2048]{1,0:T(8,128)} fusion(bf16[512,256]{1,0:T(8,128)(2,1)} %get-tuple-element.22, bf16[256,2048]{1,0:T(8,128)(2,1)S(1)} %copy-done.1), kind=kOutput, calls=%fused_computation.45 | convolution fusion | flops 536870912 | bytes 5505024 | tf_op jit(solution)/shard_map/dot_general | solution.py:31
  208.0 0.0 copy-done
  208.1 7.6 %add_convert_fusion = bf16[512,2048]{1,0:T(8,128)(2,1)} fusion(f32[512,2048]{1,0:T(8,128)} %fusion.31, bf16[512,2048]{1,0:T(8,128)(2,1)S(1)} %copy-done, bf16[512,2048]{1,0:T(8,128)(2,1)} %all-gather.6.cloned.1.call-done, bf16[2048,512]{1,0:T(8,128)(2,1)} %param.25, f32[512,512]{1,0:T(8,128)} %get-tuple-element.20, f32[512]{0:T(512)S(1)} %dynamic-slice_convert_fusion, ...), kind=kOutput, calls=%fused_computation | convolution fusion | flops 2151940096 | bytes 13635584 | tf_op jit(solution)/shard_map/dot_general | solution.py:31
  215.7 0.0 reduce-scatter.2.cloned.1.call-update
  215.7 31.6 %reduce-scatter.2.cloned.1.call-done = bf16[128,2048]{1,0:T(8,128)(2,1)} async-done(((bf16[512,2048]{1,0:T(8,128)(2,1)}), bf16[128,2048]{1,0:T(8,128)(2,1)}) %reduce-scatter.2.cloned.1.call-update) | async-done | bytes 524304 | tf_op jit(solution)/shard_map/reduce_scatter | solution.py:364
  (11 shorter events, 0.0 us)
Async XLA Ops:
  6.5 201.5 %copy-start = (bf16[512,2048]{1,0:T(8,128)(2,1)S(1)}, bf16[512,2048]{1,0:T(8,128)(2,1)}, u32[]{:S(2)}) copy-start(bf16[512,2048]{1,0:T(8,128)(2,1)} %param.38) | copy-start | bytes 6291460
  6.5 4.2 %copy-start.3 = (f32[512,2]{0,1:T(2,128)S(1)}, f32[512,2]{0,1:T(2,128)}, u32[]{:S(2)}) copy-start(f32[512,2]{0,1:T(2,128)} %param.28) | copy-start | bytes 12292
  6.5 5.1 %copy-start.2 = (bf16[2048,128]{1,0:T(8,128)(2,1)S(1)}, bf16[2048,128]{1,0:T(8,128)(2,1)}, u32[]{:S(2)}) copy-start(bf16[2048,128]{1,0:T(8,128)(2,1)} %param.31) | copy-start | bytes 1572868
  6.5 5.3 %copy-start.4 = (f32[768]{0:T(1024)S(1)}, f32[768]{0:T(1024)}, u32[]{:S(2)}) copy-start(f32[768]{0:T(1024)} %param.33) | copy-start | bytes 9220
  6.5 27.8 %all-gather.6.cloned.1.call-start = ((), (), s32[]{:S(2)}) async-start(), calls=%async_computation.1 | async-start | bytes 2621440 | tf_op jit(solution)/shard_map/all_gather | solution.py:289
  10.7 45.4 %all-gather.8.cloned.1.call-start = ((), (), s32[]{:S(2)}) async-start(), calls=%async_computation.3 | async-start | bytes 1638400 | tf_op jit(solution)/shard_map/all_gather | solution.py:291
  12.6 27.9 %copy-start.9 = (bf16[2048,64]{0,1:T(8,128)(2,1)S(1)}, bf16[2048,64]{0,1:T(8,128)(2,1)}, u32[]{:S(2)}) copy-start(bf16[2048,64]{0,1:T(8,128)(2,1)} %param.32) | copy-start | bytes 786436
  37.8 126.8 %all-gather.10.cloned.1.call-start = ((), (), s32[]{:S(2)}) async-start(), calls=%async_computation.4 | async-start | bytes 7520256 | tf_op jit(solution)/shard_map/all_gather | solution.py:324
  40.5 3.3 %copy-start.6 = (bf16[512,2048]{1,0:T(8,128)(2,1)S(1)}, bf16[512,2048]{1,0:T(8,128)(2,1)}, u32[]{:S(2)}) copy-start(bf16[512,2048]{1,0:T(8,128)(2,1)} %all-gather.6.cloned.1.call-done) | copy-start | bytes 6291460
  40.5 3.3 %copy-start.7 = (bf16[2048,256]{1,0:T(8,128)(2,1)S(1)}, bf16[2048,256]{1,0:T(8,128)(2,1)}, u32[]{:S(2)}) copy-start(bf16[2048,256]{1,0:T(8,128)(2,1)} %param.22) | copy-start | bytes 3145732
  43.7 1.4 copy-start.8
  45.2 1.9 copy-start.5
  63.7 183.7 %reduce-scatter.2.cloned.1.call-start = ((), (), s32[]{:S(2)}) async-start(), calls=%async_computation.2 | async-start | bytes 2621440 | tf_op jit(solution)/shard_map/reduce_scatter | solution.py:364
  164.5 39.9 %copy-start.1 = (bf16[256,2048]{1,0:T(8,128)(2,1)S(1)}, bf16[256,2048]{1,0:T(8,128)(2,1)}, u32[]{:S(2)}) copy-start(bf16[256,2048]{1,0:T(8,128)(2,1)} %param.39) | copy-start | bytes 3145732
Sparse Core Ops, SparseCore 0:
  10.8 23.5 all-gather.5
  37.9 18.1 all-gather.7
  63.8 100.6 all-gather.9
  215.8 31.4 reduce-scatter.1

commit v2 on v1

v2 whole, which is shorter than its diff:
```python
import functools
import math

import jax
import jax.numpy as jnp
from jax import lax
from jax.experimental import pallas as pl
from jax.experimental.pallas import tpu as pltpu
from jax.sharding import PartitionSpec as P

MEMORY_HEADS = 8
M_QK = 128
M_V = 256
PLAIN_CHANNELS = 128
ROTARY_CHANNELS = 64
VALUE_CHANNELS = 128
HEAD_WIDTH = PLAIN_CHANNELS + ROTARY_CHANNELS
SMALL_CONSTANT = 1e-06
SOFTCAP = 15.0
ROTARY_BASE = 10000.0
FAR_BELOW = -1e30
EXTRA_ROWS = 16
F32 = jnp.float32
BF16 = jnp.bfloat16
VMEM_LIMIT = 56 * 1024 * 1024
NT = (((1,), (1,)), ((), ()))
TN = (((0,), (0,)), ((), ()))


def dot(a, b):
    return jnp.dot(a, b, preferred_element_type=F32)


def rms_scale(values, gain):
    widened = values.astype(F32)
    return (
        widened
        * lax.rsqrt(jnp.mean(widened * widened, axis=-1, keepdims=True) + SMALL_CONSTANT)
        * gain.astype(F32)
    )


def split3(value):
    high = value.astype(BF16)
    rest = value - high.astype(F32)
    middle = rest.astype(BF16)
    low = (rest - middle.astype(F32)).astype(BF16)
    return high, middle, low


def local_memory(heads, query_ref, key_ref, value_ref, small_ref, shift_ref,
                 num_ref, stats_ref, state_ref):
    length = query_ref.shape[0]
    scale = M_QK ** -0.5
    gate = small_ref[:, ROTARY_CHANNELS:ROTARY_CHANNELS + heads]
    forget = small_ref[:, ROTARY_CHANNELS + heads:ROTARY_CHANNELS + 2 * heads] + shift_ref[...]
    gate = SOFTCAP * jnp.tanh(gate / SOFTCAP)
    capped = SOFTCAP * jnp.tanh(forget / SOFTCAP)
    log_forget = jnp.minimum(capped, 0.0) - jnp.log1p(jnp.exp(-jnp.abs(capped)))
    row = lax.broadcasted_iota(jnp.int32, (length, length), 0)
    col = lax.broadcasted_iota(jnp.int32, (length, length), 1)
    causal = col <= row
    cumulative = jnp.dot(
        causal.astype(F32), log_forget, preferred_element_type=F32,
        precision=lax.Precision.HIGHEST,
    )
    offset = gate - cumulative
    lanes = jnp.concatenate(
        [offset, jnp.zeros((length, 128 - heads), F32)], axis=1
    )
    offset_rows = lanes.T
    stats = []
    extras = []
    for h in range(heads):
        q = query_ref[:, h * M_QK:(h + 1) * M_QK]
        k = key_ref[:, h * M_QK:(h + 1) * M_QK]
        v = value_ref[:, h * M_V:(h + 1) * M_V]
        b = cumulative[:, h:h + 1]
        w = offset_rows[h:h + 1, :]
        masked = jnp.where(causal, w, -jnp.inf)
        top = jnp.max(masked, axis=1, keepdims=True)
        weight = jnp.exp(masked - top)
        affinity = lax.dot_general(q, k, NT, preferred_element_type=F32) * (weight * scale)
        num_ref[:, h * M_V:(h + 1) * M_V] = dot(affinity.astype(BF16), v)
        stats += [b, b + top, jnp.sum(affinity, axis=1, keepdims=True)]
        last = b[length - 1:length, :]
        best = top[length - 1:length, :]
        decay = jnp.exp(offset[:, h:h + 1] - best) * scale
        state_ref[h * M_V:(h + 1) * M_V, :] = lax.dot_general(
            (decay * v.astype(F32)).astype(BF16), k, TN, preferred_element_type=F32
        ).astype(BF16)
        normal = jnp.sum(decay * k.astype(F32), axis=0, keepdims=True)
        parts = split3(normal) + split3(jnp.broadcast_to(last + best, (1, 128))) + split3(
            jnp.broadcast_to(last, (1, 128))
        )
        extras += [part.astype(F32) for part in parts]
    stats_ref[...] = jnp.concatenate(
        stats + [jnp.zeros((length, 128 - 3 * heads), F32)], axis=1
    )
    count = len(extras)
    rows = state_ref.shape[0] - heads * M_V
    state_ref[heads * M_V:, :] = jnp.concatenate(
        extras + [jnp.zeros((rows - count, 128), F32)], axis=0
    ).astype(BF16)


def rotated(values, cosine, sine):
    half = values.shape[-1] // 2
    widened = values.astype(F32)
    first = widened[:, :half]
    second = widened[:, half:]
    return jnp.concatenate(
        [first * cosine - second * sine, second * cosine + first * sine], axis=1
    ).astype(BF16)


def prepare(heads, latents_ref, small_ref, cos_ref, sin_ref, qgain_ref, lgain_ref,
            qup_ref, query_ref, latn_ref):
    shares, length, _ = latents_ref.shape
    lat_part = lgain_ref.shape[1]
    q_part = qgain_ref.shape[1]
    lat_sum = 0.0
    q_sum = 0.0
    for t in range(shares):
        a = latents_ref[t, :, :lat_part].astype(F32)
        b = latents_ref[t, :, lat_part:].astype(F32)
        lat_sum = lat_sum + jnp.sum(a * a, axis=1, keepdims=True)
        q_sum = q_sum + jnp.sum(b * b, axis=1, keepdims=True)
    lat_rs = lax.rsqrt(lat_sum / (shares * lat_part) + SMALL_CONSTANT)
    q_rs = lax.rsqrt(q_sum / (shares * q_part) + SMALL_CONSTANT)
    query = 0.0
    for t in range(shares):
        a = latents_ref[t, :, :lat_part].astype(F32)
        b = latents_ref[t, :, lat_part:].astype(F32)
        latn_ref[:, t * lat_part:(t + 1) * lat_part] = (a * lat_rs * lgain_ref[t:t + 1, :]).astype(BF16)
        b = (b * q_rs * qgain_ref[t:t + 1, :]).astype(BF16)
        query = query + dot(b, qup_ref[t * q_part:(t + 1) * q_part, :])
    query = query.astype(BF16)
    cosine = cos_ref[...]
    sine = sin_ref[...]
    for h in range(heads):
        base = h * HEAD_WIDTH
        query_ref[h, :, :PLAIN_CHANNELS] = query[:, base:base + PLAIN_CHANNELS]
        query_ref[h, :, PLAIN_CHANNELS:] = rotated(
            query[:, base + PLAIN_CHANNELS:base + HEAD_WIDTH], cosine, sine
        )
    latn_ref[:, shares * lat_part:] = rotated(
        small_ref[:, :ROTARY_CHANNELS].astype(BF16), cosine, sine
    )


def mixers(mem_heads, att_heads, nz, nx, tp,
           latn_ref, state_ref, query_ref, kup_ref, vup_ref, memq_ref, num_ref, stats_ref,
           cell_ref, square_ref, attended_ref,
           lat_ref, states_ref, top_ref, sum_ref, acc_ref, matrix_ref, normal_ref, stab_ref,
           recv_l, recv_s, send_lz, send_sz, send_lx, send_sx, send_ly, send_lc):
    mine = lax.axis_index("sp")
    t = lax.axis_index("tp")
    z = mine // nx
    x = lax.rem(mine, nx)
    ny = tp // 2
    y = t // 2
    core = lax.rem(t, 2)
    sibling = y * 2 + 1 - core
    length = query_ref.shape[1]
    rows = length // tp
    rank = latn_ref.shape[1] - ROTARY_CHANNELS
    factor = HEAD_WIDTH ** -0.5

    barrier = pltpu.get_barrier_semaphore()
    friends = [(mine, sibling)]
    if nz > 1:
        friends += [(lax.rem(z + 1, nz) * nx + x, t), (lax.rem(z + nz - 1, nz) * nx + x, t)]
    friends += [(z * nx + lax.rem(x + j, nx), t) for j in range(1, nx)]
    friends += [(mine, lax.rem(y + j, ny) * 2 + core) for j in range(1, ny)]
    for friend in friends:
        pl.semaphore_signal(barrier, inc=1, device_id=friend, device_id_type=pl.DeviceIdType.MESH)
    pl.semaphore_wait(barrier, len(friends))

    def remote(src, dst, send, recv, target):
        return pltpu.make_async_remote_copy(
            src_ref=src, dst_ref=dst, send_sem=send, recv_sem=recv, device_id=target,
            device_id_type=pl.DeviceIdType.MESH,
        )

    up = lax.rem(z + 1, nz) * nx + x
    own = latn_ref.at[pl.ds(pl.multiple_of(t * rows, rows), rows)]

    def quarter(slot, own_block):
        return own if own_block else lat_ref.at[slot, t]

    def state_of(slot, own_block):
        return state_ref if own_block else states_ref.at[slot]

    def to_up(slot, own_block=False):
        return [
            remote(state_of(slot, own_block), states_ref.at[slot], send_sz.at[slot],
                   recv_s.at[slot], (up, t)),
            remote(quarter(slot, own_block), lat_ref.at[slot, t], send_lz.at[slot],
                   recv_l.at[slot, t], (up, t)),
        ]

    def to_side(slot, j, own_block=False):
        target = (z * nx + lax.rem(x + j, nx), t)
        return [
            remote(state_of(slot, own_block), states_ref.at[slot], send_sx.at[slot, j],
                   recv_s.at[slot], target),
            remote(quarter(slot, own_block), lat_ref.at[slot, t], send_lx.at[slot, j],
                   recv_l.at[slot, t], target),
        ]

    def to_peer(slot, j):
        return remote(lat_ref.at[slot, t], lat_ref.at[slot, t], send_ly.at[slot, j],
                      recv_l.at[slot, t], (mine, lax.rem(y + j, ny) * 2 + core))

    def to_sibling(slot, part):
        return remote(lat_ref.at[slot, part], lat_ref.at[slot, part], send_lc.at[slot, part],
                      recv_l.at[slot, part], (mine, sibling))

    def landed(slot, part):
        remote(lat_ref.at[slot, part], lat_ref.at[slot, part], send_lc.at[slot, part],
               recv_l.at[slot, part], (mine, sibling)).wait_recv()

    def start(copies):
        for copy in copies:
            copy.start()

    def sent(copies):
        for copy in copies:
            copy.wait_send()

    def each_own(action):
        @pl.when(z < nz - 1)
        def _():
            action(to_up(mine, True))
        for j in range(1, nx):
            @pl.when(x + j < nx)
            def _():
                action(to_side(mine, j, True))

    def each_column(slot, action):
        for j in range(1, nx):
            action(to_side(slot, j))
        @pl.when(z < nz - 1)
        def _():
            action(to_up(slot))

    def each_handled(slot, action):
        action([to_peer(slot, j) for j in range(1, ny)] + [to_sibling(slot, t)])

    def arrive(slot):
        remote(states_ref.at[slot], states_ref.at[slot], send_sz.at[slot], recv_s.at[slot],
               (mine, sibling)).wait_recv()
        landed(slot, t)

    each_own(start)

    top_ref[...] = jnp.full(top_ref.shape, FAR_BELOW, F32)
    sum_ref[...] = jnp.zeros(sum_ref.shape, F32)
    acc_ref[...] = jnp.zeros(acc_ref.shape, F32)
    matrix_ref[...] = jnp.zeros(matrix_ref.shape, F32)
    normal_ref[...] = jnp.zeros(normal_ref.shape, F32)
    stab_ref[...] = jnp.zeros(stab_ref.shape, F32)

    def attend(block, masked):
        latent = block[:, :rank]
        rotary = block[:, rank:]
        keys = dot(latent, kup_ref[...]).astype(BF16)
        values = dot(latent, vup_ref[...]).astype(BF16)
        for h in range(att_heads):
            key = jnp.concatenate(
                [keys[:, h * PLAIN_CHANNELS:(h + 1) * PLAIN_CHANNELS], rotary], axis=1
            )
            scores = lax.dot_general(query_ref[h], key, NT, preferred_element_type=F32)
            if masked:
                row = lax.broadcasted_iota(jnp.int32, scores.shape, 0)
                col = lax.broadcasted_iota(jnp.int32, scores.shape, 1)
                scores = jnp.where(col <= row, scores, FAR_BELOW)
            old = top_ref[h, :, :1]
            new = jnp.maximum(old, jnp.max(scores, axis=1, keepdims=True))
            probs = jnp.exp((scores - new) * factor)
            shrink = jnp.exp((old - new) * factor)
            sum_ref[h] = sum_ref[h] * shrink + jnp.sum(probs, axis=1, keepdims=True)
            value = values[:, h * VALUE_CHANNELS:(h + 1) * VALUE_CHANNELS]
            acc_ref[h] = acc_ref[h] * shrink + dot(probs.astype(BF16), value)
            top_ref[h] = jnp.broadcast_to(new, top_ref.shape[1:])

    attend(latn_ref[...], True)

    def handle_column(slot):
        arrive(slot)
        each_column(slot, start)
        each_handled(slot, start)

    def handle_side(slot):
        arrive(slot)
        each_handled(slot, start)

    def finish(slot):
        for j in range(1, ny):
            part = lax.rem(y + j, ny) * 2 + core
            landed(slot, part)
            to_sibling(slot, part).start()
        for j in range(ny):
            landed(slot, lax.rem(y + j, ny) * 2 + 1 - core)
        attend(lat_ref[slot].reshape(length, rank + ROTARY_CHANNELS), False)

    def clean(slot, column):
        if column:
            each_column(slot, sent)
        each_handled(slot, sent)
        for j in range(1, ny):
            to_sibling(slot, lax.rem(y + j, ny) * 2 + core).wait_send()

    def side_slots(d, act):
        for j in range(1, nx):
            other = lax.rem(x + j, nx)

            @pl.when(jnp.logical_and(jnp.logical_and(d >= 0, d <= z),
                                     jnp.logical_or(d > 0, other < x)))
            def _():
                act((z - d) * nx + other)

    def round_(d, carry):
        @pl.when(d <= z)
        def _():
            handle_column((z - d) * nx + x)
        side_slots(d - 2, finish)
        side_slots(d - 1, handle_side)
        @pl.when(d <= z)
        def _():
            finish((z - d) * nx + x)
        return carry

    lax.fori_loop(1, z + 3, round_, 0)

    for h in range(att_heads):
        attended_ref[:, h * VALUE_CHANNELS:(h + 1) * VALUE_CHANNELS] = (
            acc_ref[h] / sum_ref[h]
        ).astype(BF16)

    def fold(k, carry):
        extra = states_ref[k, mem_heads * M_V:, :].astype(F32)
        state = states_ref[k, :mem_heads * M_V, :].astype(F32)
        pieces = [extra[9 * h + 3 * g:9 * h + 3 * g + 1] + extra[9 * h + 3 * g + 1:9 * h + 3 * g + 2]
                  + extra[9 * h + 3 * g + 2:9 * h + 3 * g + 3]
                  for h in range(mem_heads) for g in range(3)]
        for h in range(mem_heads):
            normal, best, last = pieces[3 * h:3 * h + 3]
            decayed = stab_ref[h:h + 1, :] + last
            new = jnp.maximum(decayed, best)
            early = jnp.exp(decayed - new)
            late = jnp.exp(best - new)
            span = slice(h * M_V, (h + 1) * M_V)
            matrix_ref[span, :] = matrix_ref[span, :] * early + late * state[span, :]
            normal_ref[h:h + 1, :] = normal_ref[h:h + 1, :] * early + late * normal
            stab_ref[h:h + 1, :] = new
        return carry

    lax.fori_loop(0, mine, fold, 0)

    squares = 0.0
    for h in range(mem_heads):
        b = stats_ref[:, 3 * h:3 * h + 1]
        local = stats_ref[:, 3 * h + 1:3 * h + 2]
        local_den = stats_ref[:, 3 * h + 2:3 * h + 3]
        q = memq_ref[:, h * M_QK:(h + 1) * M_QK]
        carried = b + stab_ref[h:h + 1, :1]
        row_max = jnp.maximum(carried, local)
        across = jnp.exp(carried - row_max)
        within = jnp.exp(local - row_max)
        inter = lax.dot_general(
            q, matrix_ref[h * M_V:(h + 1) * M_V, :].astype(BF16), NT,
            preferred_element_type=F32,
        )
        dots = jnp.sum(q.astype(F32) * normal_ref[h:h + 1, :], axis=1, keepdims=True)
        den = within * local_den + across * dots
        den = jnp.maximum(jnp.abs(den), jnp.exp(-row_max))
        cell = (within * num_ref[:, h * M_V:(h + 1) * M_V] + across * inter) / den
        cell_ref[:, h * M_V:(h + 1) * M_V] = cell
        squares = squares + jnp.sum(cell * cell, axis=1, keepdims=True)
    square_ref[...] = jnp.broadcast_to(squares, (length, 128)).T[:8]

    each_own(sent)

    def tidy(d, carry):
        @pl.when(d > 0)
        def _():
            clean((z - d) * nx + x, True)
        side_slots(d, lambda slot: clean(slot, False))
        return carry

    lax.fori_loop(0, z + 1, tidy, 0)


def project_out(tp, heads_total, cell_ref, square_ref, gate_ref, gain_ref, attended_ref,
                memory_ref, attend_ref, out_ref,
                gated_ref, squares_ref, held_ref, sib_ref, send_ref, far_ref,
                recv_q, send_q, recv_c, send_c, recv_f, send_f):
    mine = lax.axis_index("sp")
    t = lax.axis_index("tp")
    ny = tp // 2
    y = t // 2
    core = lax.rem(t, 2)
    sibling = y * 2 + 1 - core
    rows = out_ref.shape[0]
    barrier = pltpu.get_barrier_semaphore()
    for j in range(1, tp):
        pl.semaphore_signal(barrier, inc=1, device_id=(mine, lax.rem(t + j, tp)),
                            device_id_type=pl.DeviceIdType.MESH)
    pl.semaphore_wait(barrier, tp - 1)

    def remote(src, dst, send, recv, target):
        return pltpu.make_async_remote_copy(
            src_ref=src, dst_ref=dst, send_sem=send, recv_sem=recv, device_id=(mine, target),
            device_id_type=pl.DeviceIdType.MESH,
        )

    copies = [
        remote(square_ref, squares_ref.at[j - 1], send_q.at[j - 1], recv_q.at[j - 1],
               lax.rem(t + j, tp)) for j in range(1, tp)
    ]
    for copy in copies:
        copy.start()
    for copy in copies:
        copy.wait()
    total = square_ref[...]
    for j in range(tp - 1):
        total = total + squares_ref[j]
    total = jnp.concatenate([total] * 16, axis=0).T[:, :1]
    scale = lax.rsqrt(total / (heads_total * M_V) + SMALL_CONSTANT)
    opened = jax.nn.sigmoid(gate_ref[...].astype(F32))
    gated_ref[...] = (cell_ref[...] * scale * gain_ref[...].astype(F32) * opened).astype(BF16)

    def partial(owner):
        span = pl.ds(pl.multiple_of(owner * rows, rows), rows)
        return (
            dot(gated_ref[span, :], memory_ref[...]) + dot(attended_ref[span, :], attend_ref[...])
        ).astype(BF16)

    def to_sibling(j):
        return remote(held_ref.at[j], sib_ref.at[j], send_c.at[j], recv_c.at[j], sibling)

    def to_far(j):
        return remote(send_ref.at[j - 1], far_ref.at[j - 1], send_f.at[j - 1], recv_f.at[j - 1],
                      lax.rem(y + j, ny) * 2 + core)

    order = list(range(1, ny)) + [0]
    for j in order:
        chip = lax.rem(y + j, ny) * 2
        held_ref[j] = partial(chip + 1 - core)
        to_sibling(j).start()
        result = partial(chip + core).astype(F32)
        to_sibling(j).wait_recv()
        result = result + sib_ref[j].astype(F32)
        if j:
            send_ref[j - 1] = result.astype(BF16)
            to_far(j).start()
    for j in range(1, ny):
        to_far(j).wait_recv()
        result = result + far_ref[j - 1].astype(F32)
    out_ref[...] = result.astype(BF16)
    for j in order:
        to_sibling(j).wait_send()
    for j in range(1, ny):
        to_far(j).wait_send()


def params(**more):
    return pltpu.CompilerParams(vmem_limit_bytes=VMEM_LIMIT, **more)


def per_device(
    nx, tokens, input_gain, weight_query, weight_key, weight_value, weight_outgate, weight_ingate,
    weight_forget, forget_shift, mem_gain, query_down_weight, latent_down_weight, down_rotary,
    query_gain, latent_gain, query_up_weight, key_up_weight, value_up_weight, out_memory,
    out_attend,
):
    tp_index = lax.axis_index("tp")
    tp = lax.axis_size("tp")
    sp = lax.axis_size("sp")
    mem_heads = weight_query.shape[1] // M_QK
    att_heads = key_up_weight.shape[1] // PLAIN_CHANNELS
    length = tokens.shape[0] * tp
    model = tokens.shape[1]
    ingate_cols = lax.dynamic_slice_in_dim(weight_ingate, tp_index * mem_heads, mem_heads, 1)
    forget_cols = lax.dynamic_slice_in_dim(weight_forget, tp_index * mem_heads, mem_heads, 1)
    small_weight = jnp.concatenate(
        [down_rotary, ingate_cols, forget_cols,
         jnp.zeros((model, 128 - ROTARY_CHANNELS - 2 * mem_heads), BF16)], axis=1
    )
    latent_weight = jnp.concatenate([latent_down_weight, query_down_weight], axis=1)
    positions = lax.axis_index("sp") * length + jnp.arange(length, dtype=jnp.int32)
    half = ROTARY_CHANNELS // 2
    inverse = jnp.power(ROTARY_BASE, -jnp.arange(half, dtype=F32) / half)
    angles = positions.astype(F32)[:, None] * inverse
    cosine = jnp.cos(angles)
    sine = jnp.sin(angles)

    normed = rms_scale(tokens, input_gain).astype(BF16)
    rows = lax.all_gather(normed, "tp", axis=0, tiled=True)
    latents = dot(rows, latent_weight).astype(BF16)
    latents_all = lax.all_gather(latents, "tp", axis=0)
    small = dot(rows, small_weight)
    mem_query = dot(rows, weight_query).astype(BF16)
    mem_key = dot(rows, weight_key).astype(BF16)
    mem_value = dot(rows, weight_value).astype(BF16)
    mem_outgate = dot(rows, weight_outgate).astype(BF16)

    extra_rows = -(-9 * mem_heads // 32) * 32
    num, stats, state = pl.pallas_call(
        functools.partial(local_memory, mem_heads),
        out_shape=(
            jax.ShapeDtypeStruct((length, mem_heads * M_V), F32),
            jax.ShapeDtypeStruct((length, 128), F32),
            jax.ShapeDtypeStruct((mem_heads * M_V + extra_rows, 128), BF16),
        ),
        compiler_params=params(),
        name="local_memory",
    )(mem_query, mem_key, mem_value, small, forget_shift)

    query, latn = pl.pallas_call(
        functools.partial(prepare, att_heads),
        out_shape=(
            jax.ShapeDtypeStruct((att_heads, length, HEAD_WIDTH), BF16),
            jax.ShapeDtypeStruct((length, key_up_weight.shape[0] + ROTARY_CHANNELS), BF16),
        ),
        compiler_params=params(),
        name="prepare",
    )(
        latents_all, small, cosine, sine, query_gain.reshape(tp, -1), latent_gain.reshape(tp, -1),
        query_up_weight,
    )

    dma = pltpu.SemaphoreType.DMA
    cell, squares, attended = pl.pallas_call(
        functools.partial(mixers, mem_heads, att_heads, sp // nx, nx, tp),
        out_shape=(
            jax.ShapeDtypeStruct((length, mem_heads * M_V), F32),
            jax.ShapeDtypeStruct((8, length), F32),
            jax.ShapeDtypeStruct((length, att_heads * VALUE_CHANNELS), BF16),
        ),
        scratch_shapes=[
            pltpu.VMEM((sp, tp, length // tp, latn.shape[1]), BF16),
            pltpu.VMEM((sp,) + state.shape, BF16),
            pltpu.VMEM((att_heads, length, 128), F32),
            pltpu.VMEM((att_heads, length, 128), F32),
            pltpu.VMEM((att_heads, length, VALUE_CHANNELS), F32),
            pltpu.VMEM((mem_heads * M_V, 128), F32),
            pltpu.VMEM((8, 128), F32),
            pltpu.VMEM((8, 128), F32),
            dma((sp, tp)), dma((sp,)), dma((sp,)), dma((sp,)),
            dma((sp, nx)), dma((sp, nx)), dma((sp, tp // 2)), dma((sp, tp)),
        ],
        compiler_params=params(collective_id=1, has_side_effects=True),
        name="mixers",
    )(latn, state, query, key_up_weight, value_up_weight, mem_query, num, stats)

    gain_part = lax.dynamic_slice_in_dim(mem_gain, tp_index * mem_heads * M_V, mem_heads * M_V, 0)
    block = (length // tp, out_memory.shape[1])
    ny = tp // 2
    far = max(ny - 1, 1)
    return pl.pallas_call(
        functools.partial(project_out, tp, tp * mem_heads),
        out_shape=jax.ShapeDtypeStruct(block, BF16),
        scratch_shapes=[
            pltpu.VMEM((length, mem_heads * M_V), BF16),
            pltpu.VMEM((tp - 1, 8, length), F32),
            pltpu.VMEM((ny,) + block, BF16),
            pltpu.VMEM((ny,) + block, BF16),
            pltpu.VMEM((far,) + block, BF16),
            pltpu.VMEM((far,) + block, BF16),
            dma((tp - 1,)), dma((tp - 1,)), dma((ny,)), dma((ny,)), dma((far,)), dma((far,)),
        ],
        compiler_params=params(collective_id=2, has_side_effects=True),
        name="project_out",
    )(cell, squares, mem_outgate, gain_part.reshape(1, -1), attended, out_memory, out_attend)


def solution(mesh):
    placed = (
        P(("sp", "tp"), None), P(), P(None, "tp"), P(None, "tp"), P(None, "tp"), P(None, "tp"),
        P(), P(), P("sp", "tp"), P(), P(None, "tp"), P(None, "tp"), P(), P(), P(),
        P(None, "tp"), P(None, "tp"), P(None, "tp"), P("tp", None), P("tp", None),
    )
    nx = len({getattr(d, "coords", (0,))[0] for d in mesh.devices.flat})
    if mesh.shape["sp"] % nx:
        nx = 1
    return jax.shard_map(
        functools.partial(per_device, nx), mesh=mesh, in_specs=placed, out_specs=P(("sp", "tp"), None), check_vma=False
    )
```

time: 256 us -> 156 us (0.61)
  waiting for transfers between devices: 154 us -> 22.6 us
  Pallas kernels: 35.5 us -> 91.2 us
  blocking collectives: 15.1 us -> 0 us
  matrix products: 22.7 us -> 13.5 us
  local copies, waits for them, and re-layouts: 5.68 us -> 8.47 us
    all_gather x1 -> x0, waiting for transfers between devices: 99.8 us -> none  [per_device(): packs = lax.all_gather(pack, 'sp', axis=0)]
    pallas_call x1 -> x2, Pallas kernels: 24.6 us -> 80.4 us  [the longest x1 57.1 us: per_device(): pl.pallas_call(functools.partial(mixers, mem_heads, att_heads, sp // nx,...]
    reduce_scatter x1 -> x0, waiting for transfers between devices: 31.6 us -> none  [per_device(): return lax.psum_scatter(partial, 'tp', scatter_dimension=0, tiled=True)]
    psum x1 -> x0, blocking collectives: 15.1 us -> none  [per_device(): total = lax.psum(squares, 'tp')]
    dot_general x7 -> x6, matrix products: 22.7 us -> 13.5 us  [dot(): return jnp.dot(a, b, preferred_element_type=F32)]
  transfers between devices with their start and end apart: 4 -> 2, of which waited for: 4 -> 1; matrix products, arithmetic and copies ran while one was open for 5% -> 10% of each run, Pallas kernels for 2% -> 4%
where the time goes in v2:
time: 156 us; the launch traced here: 155 us
  Pallas kernels  91.2 us (58%)
  waiting for transfers between devices  22.6 us (14%)
  matrix products  13.5 us (9%)
  between operations  13.5 us (9%)
  local copies, waits for them, and re-layouts  8.47 us (5%)
  other arithmetic  5.91 us (4%)
    pallas_call x1, Pallas kernels, per_device(): pl.pallas_call(functools.partial(mixers, mem_heads, att_heads, sp // nx,...  57.1 us
    pallas_call x1, Pallas kernels, per_device(): pl.pallas_call(functools.partial(project_out, tp, tp * mem_heads), out_sh...  23.3 us
    all_gather x1, waiting for transfers between devices, per_device(): rows = lax.all_gather(normed, 'tp', axis=0, tiled=True)  22.5 us
    dot_general x6, matrix products, dot(): return jnp.dot(a, b, preferred_element_type=F32)  13.5 us
    pallas_call x1, Pallas kernels, per_device(): pl.pallas_call(functools.partial(local_memory, mem_heads), out_shape=(jax...  5.91 us
    pallas_call x1, Pallas kernels, per_device(): pl.pallas_call(functools.partial(prepare, att_heads), out_shape=(jax.Shap...  4.86 us
  transfers between devices with their start and end apart: 2, of which 1 were waited for; matrix products, arithmetic and copies ran while one was open for 10% of the time, Pallas kernels for 4%

profile of v2, /device:TPU:26, one launch (start us, length us, event | category | flops | bytes accessed | tf_op | source)
XLA Modules:
  0.0 155.2 jit_solution(11415115862277970136)
XLA Ops:
  6.5 0.0 copy-start
  6.5 0.0 copy-start.1
  6.5 0.0 all-gather.4.cloned.1.call-start
  6.5 1.4 fusion.7
  7.9 0.7 convert_element_type.32
  8.6 2.0 %fusion.9 = bf16[128,2048]{1,0:T(8,128)(2,1)} fusion(bf16[128,2048]{1,0:T(8,128)(2,1)} %param.20, f32[2048]{0:T(1024)S(1)} %convert_element_type.32, f32[128]{0:T(128)S(1)} %add_rsqrt_fusion), kind=kLoop, calls=%fused_computation.13 | loop fusion | flops 1048576 | bytes 1057280 | tf_op jit(solution)/shard_map/convert_element_type | solution.py:500
  10.6 0.0 all-gather.4.cloned.1.call-update
  10.7 0.0 all-gather.6.cloned.1.call-start
  10.7 0.0 copy-done.1
  10.7 0.2 copy.24
  11.0 0.8 constant_dynamic-slice_fusion
  11.8 0.0 copy-start.3
  11.8 0.0 copy-start.2
  11.8 0.0 copy-start.8
  11.8 22.5 %all-gather.4.cloned.1.call-done = bf16[512,2048]{1,0:T(8,128)(2,1)} async-done(((bf16[128,2048]{1,0:T(8,128)(2,1)}), bf16[512,2048]{1,0:T(8,128)(2,1)}) %all-gather.4.cloned.1.call-update) | async-done | bytes 2097168 | tf_op jit(solution)/shard_map/all_gather | solution.py:501
  34.3 3.4 %fusion.4 = bf16[512,320]{0,1:T(8,128)(2,1)} fusion(bf16[512,2048]{1,0:T(8,128)(2,1)} %all-gather.4.cloned.1.call-done, bf16[2048,192]{0,1:T(8,128)(2,1)} %param.30, bf16[2048,128]{0,1:T(8,128)(2,1)S(1)} %copy.24), kind=kOutput, calls=%fused_computation.8 | convolution fusion | flops 673873920 | bytes 3735552 | tf_op jit(solution)/shard_map/dot_general | solution.py:31
  37.7 0.0 all-gather.6.cloned.1.call-update
  37.7 0.8 dynamic_slice.11
  38.5 0.6 reshape.31.gain_ref
  39.1 0.0 copy-done.3
  39.1 0.7 reshape.29.qgain_ref
  39.8 0.0 copy-done.2
  39.8 0.9 copy.27.shift_ref
  40.6 0.1 pad.3.clone
  40.7 1.8 %multiply_sine_fusion = (f32[512,32]{1,0:T(8,128)}, f32[512,32]{1,0:T(8,128)}) fusion(f32[512]{0:T(512)S(1)} %add_convert_fusion, f32[32]{0:T(128)S(1)} %multiply_power_fusion), kind=kLoop, calls=%fused_computation.21 | loop fusion | flops 16384 | bytes 133248 | tf_op jit(solution)/shard_map/sin | solution.py:498
  42.5 0.0 copy-done.8
  42.5 0.0 copy-start.5
  42.5 0.0 copy-start.6
  42.5 3.3 %fusion.10.small_ref = f32[512,128]{1,0:T(8,128)} fusion(bf16[512,2048]{1,0:T(8,128)(2,1)} %all-gather.4.cloned.1.call-done, bf16[2048,2]{0,1:T(2,128)(2,1)S(1)} %get-tuple-element.23, bf16[2048,2]{0,1:T(2,128)(2,1)S(1)} %get-tuple-element.24, bf16[2048,64]{0,1:T(8,128)(2,1)S(1)} %copy-done.8, bf16[128]{0:T(256)(128)(2,1)S(1)} %pad.3.clone), kind=kOutput, calls=%fused_computation.14 | convolution fusion | flops 270532608 | bytes 2638080 | tf_op jit(solution)/shard_map/dot_general | solution.py:31
  45.8 0.0 copy-done.5
  45.8 0.0 copy-done.6
  45.8 0.0 copy-start.7
  45.8 1.4 convolution_convert_fusion.3.query_ref.memq_ref
  47.2 0.0 copy-done.7
  47.2 1.4 convolution_convert_fusion.2.key_ref
  48.6 0.0 copy-done
  48.6 0.0 copy-start.4
  48.6 2.0 %convolution_convert_fusion.1.value_ref = bf16[512,512]{1,0:T(8,128)(2,1)} fusion(bf16[512,2048]{1,0:T(8,128)(2,1)S(1)} %copy-done.5, bf16[2048,512]{1,0:T(8,128)(2,1)S(1)} %copy-done), kind=kOutput, calls=%fused_computation.7 | convolution fusion | flops 1074003968 | bytes 4718592 | tf_op jit(solution)/shard_map/dot_general | solution.py:31
  50.7 5.9 %local_memory.1 = (f32[512,512]{1,0:T(8,128)}, f32[512,128]{1,0:T(8,128)}, bf16[544,128]{1,0:T(8,128)(2,1)}) custom-call(bf16[512,256]{1,0:T(8,128)(2,1)} %convolution_convert_fusion.3.query_ref.memq_ref, bf16[512,256]{1,0:T(8,128)(2,1)} %convolution_convert_fusion.2.key_ref, bf16[512,512]{1,0:T(8,128)(2,1)} %convolution_convert_fusion.1.value_ref, ...), custom_call_target="tpu_custom_call" | custom-call | tf_op jit(solution)/shard_map/local_memory/pallas_call | solution.py:511
  56.6 0.0 copy-done.4
  56.6 2.1 %convolution_convert_fusion.gate_ref = bf16[512,512]{1,0:T(8,128)(2,1)} fusion(bf16[512,2048]{1,0:T(8,128)(2,1)S(1)} %copy-done.5, bf16[2048,512]{1,0:T(8,128)(2,1)S(1)} %copy-done.4), kind=kOutput, calls=%fused_computation.6 | convolution fusion | flops 1074003968 | bytes 4718592 | tf_op jit(solution)/shard_map/dot_general | solution.py:31
  58.6 0.0 all-gather.6.cloned.1.call-done
  58.6 2.6 %copy.25 = bf16[2048,320]{1,0:T(8,128)(2,1)} copy(bf16[2048,320]{0,1:T(8,128)(2,1)} %all-gather.6.cloned.1.call-done) | data formatting | bytes 2621440 | tf_op jit(solution)/shard_map/all_gather | solution.py:503
  61.2 4.9 %prepare.1 = (bf16[2,512,192]{2,1,0:T(8,128)(2,1)}, bf16[512,576]{1,0:T(8,128)(2,1)}) custom-call(bf16[4,512,320]{2,1,0:T(8,128)(2,1)} %bitcast.12, f32[512,128]{1,0:T(8,128)} %fusion.10.small_ref, f32[512,32]{1,0:T(8,128)} %get-tuple-element.22.cos_ref, f32[512,32]{1,0:T(8,128)} %get-tuple-element.21.sin_ref, f32[4,192]{1,0:T(4,128)} %reshape.29.qgain_ref, ...), custom_call_target="tpu_custom_call" | custom-call | tf_op jit(solution)/shard_map/prepare/pallas_call | solution.py:522
  66.1 57.1 %mixers.1 = (f32[512,512]{1,0:T(8,128)}, f32[8,512]{1,0:T(8,128)}, bf16[512,256]{1,0:T(8,128)(2,1)}) custom-call(bf16[512,576]{1,0:T(8,128)(2,1)} %get-tuple-element.13.latn_ref, bf16[544,128]{1,0:T(8,128)(2,1)} %get-tuple-element.14.state_ref, bf16[2,512,192]{2,1,0:T(8,128)(2,1)} %get-tuple-element.15.query_ref, bf16[512,256]{1,0:T(8,128)(2,1)} %kup_ref.1, ...), custom_call_target="tpu_custom_call" | custom-call | tf_op jit(solution)/shard_map/mixers/pallas_call | solution.py:536
  123.2 23.3 %project_out.1 = bf16[128,2048]{1,0:T(8,128)(2,1)} custom-call(f32[512,512]{1,0:T(8,128)} %get-tuple-element.18.cell_ref, f32[8,512]{1,0:T(8,128)} %get-tuple-element.19.square_ref, bf16[512,512]{1,0:T(8,128)(2,1)} %convolution_convert_fusion.gate_ref, bf16[1,512]{1,0:T(2,128)(2,1)} %reshape.31.gain_ref, bf16[512,256]{1,0:T(8,128)(2,1)} %get-tuple-element.20.attended_ref, ...), custom_call_target="tpu_custom_call" | custom-call | tf_op jit(solution)/shard_map/project_out/pallas_call | solution.py:563
  146.5 1.9 %copy.29 = bf16[128,2048]{1,0:T(8,128)(2,1)} copy(bf16[128,2048]{1,0:T(8,128)(2,1)} %project_out.1) | data formatting | bytes 1048576
  (4 shorter events, 0.0 us)
Async XLA Ops:
  6.5 42.1 %copy-start = (bf16[2048,512]{1,0:T(8,128)(2,1)S(1)}, bf16[2048,512]{1,0:T(8,128)(2,1)}, u32[]{:S(2)}) copy-start(bf16[2048,512]{1,0:T(8,128)(2,1)} %param.24) | copy-start | bytes 6291460
  6.5 4.2 %copy-start.1 = (bf16[2048,128]{1,0:T(8,128)(2,1)S(1)}, bf16[2048,128]{1,0:T(8,128)(2,1)}, u32[]{:S(2)}) copy-start(bf16[2048,128]{1,0:T(8,128)(2,1)} %param.31) | copy-start | bytes 1572868
  6.5 27.8 %all-gather.4.cloned.1.call-start = ((), (), s32[]{:S(2)}) async-start(), calls=%async_computation | async-start | bytes 2621440 | tf_op jit(solution)/shard_map/all_gather | solution.py:501
  10.7 48.0 %all-gather.6.cloned.1.call-start = ((), (), s32[]{:S(2)}) async-start(), calls=%async_computation.1 | async-start | bytes 1638400 | tf_op jit(solution)/shard_map/all_gather | solution.py:503
  11.8 27.3 %copy-start.3 = (f32[768]{0:T(1024)S(1)}, f32[768]{0:T(1024)}, u32[]{:S(2)}) copy-start(f32[768]{0:T(1024)} %param.33) | copy-start | bytes 9220
  11.8 28.0 %copy-start.2 = (f32[512,2]{0,1:T(2,128)S(1)}, f32[512,2]{0,1:T(2,128)}, u32[]{:S(2)}) copy-start(f32[512,2]{0,1:T(2,128)} %param.28) | copy-start | bytes 12292
  11.8 30.7 %copy-start.8 = (bf16[2048,64]{0,1:T(8,128)(2,1)S(1)}, bf16[2048,64]{0,1:T(8,128)(2,1)}, u32[]{:S(2)}) copy-start(bf16[2048,64]{0,1:T(8,128)(2,1)} %param.32) | copy-start | bytes 786436
  42.5 3.3 %copy-start.5 = (bf16[512,2048]{1,0:T(8,128)(2,1)S(1)}, bf16[512,2048]{1,0:T(8,128)(2,1)}, u32[]{:S(2)}) copy-start(bf16[512,2048]{1,0:T(8,128)(2,1)} %all-gather.4.cloned.1.call-done) | copy-start | bytes 6291460
  42.5 3.3 %copy-start.6 = (bf16[2048,256]{1,0:T(8,128)(2,1)S(1)}, bf16[2048,256]{1,0:T(8,128)(2,1)}, u32[]{:S(2)}) copy-start(bf16[2048,256]{1,0:T(8,128)(2,1)} %param.22) | copy-start | bytes 3145732
  45.8 1.4 copy-start.7
  48.6 8.0 %copy-start.4 = (bf16[2048,512]{1,0:T(8,128)(2,1)S(1)}, bf16[2048,512]{1,0:T(8,128)(2,1)}, u32[]{:S(2)}) copy-start(bf16[2048,512]{1,0:T(8,128)(2,1)} %param.25) | copy-start | bytes 6291460
Sparse Core Ops, SparseCore 0:
  10.8 23.5 all-gather.3
  37.8 18.1 all-gather.5
